TPU v7x, 512 devices: a whole 4x8x8 slice. The times are simulated.
512 devices in a mesh: sp: 64 (over z, y), fs: 4 (over x), tp: 2 (over core).
Axes of the slice: x: 4, y: 8, z: 8, core: 2. Of those that a mesh axis runs over, the one named last changes fastest.
Arguments:
- tokens: bfloat16 [4, 8192, 2048], P('fs', ('sp', 'tp')), may hold values from -6 to 6
- input_norm_gain: float32 [2048], replicated, may hold values from 0.1 to 1.9
- pooling_input_weight: bfloat16 [2048, 1024], P('sp', 'tp'), may hold values from -0.125 to 0.125
- query_weight: bfloat16 [2048, 1024], P('sp', 'tp'), may hold values from -0.125 to 0.125
- forget_weight: bfloat16 [2048, 1024], P('sp', 'tp'), may hold values from -0.125 to 0.125
- value_weight: bfloat16 [2048, 1024], P('sp', 'tp'), may hold values from -0.125 to 0.125
- pooling_group_maps: bfloat16 [4, 256, 256], P('tp'), may hold values from -0.375 to 0.375
- pooling_scale: float32 [1024], P('tp'), may hold values from 0.1 to 1.9
- lower_bound_logits: float32 [1024], P('tp')
- decay_spike: float32 [4, 8192, 8], P('fs', 'sp', 'tp'), may hold values from -0.75 to 0
- head_norm_gain: float32 [1024], P('tp'), may hold values from 0.1 to 1.9
- pooling_output_weight: bfloat16 [1024, 2048], P('tp', 'sp'), may hold values from -0.125 to 0.125
- recurrent_output_weight: bfloat16 [1024, 2048], P('tp', 'sp'), may hold values from -0.125 to 0.125
Outputs:
- mixed: bfloat16 [4, 8192, 2048], P('fs', ('sp', 'tp'))
All inputs are finite; a program needn't handle non-finite values.
Results may differ from a plain program's by a relative error of at most 0.013.
Values may be sent and summed in bfloat16 or wider, within the bound.
A program may use at most 64 MiB of HBM per device.

v0:
```python
import jax
import jax.numpy as jnp
from jax import lax
from jax.sharding import Mesh
from jax.sharding import PartitionSpec as P

BLOCK = 64
SP = ("sp_0", "sp_1")
SP_TP = ("sp_0", "sp_1", "tp")


EPSILON = 1e-06
HIGHEST = lax.Precision.HIGHEST


def in_order(tiles, dim):
    tiles = jnp.moveaxis(tiles, 0, dim)
    dims = tiles.shape
    return tiles.reshape(*dims[:dim], dims[dim] * dims[dim + 1], *dims[dim + 2 :])


def all_blocks(shard, axes, sequence):
    tiles = shard
    for k in sequence:
        tiles = lax.all_gather(tiles, axes[k])
    done = sequence[::-1]
    back = [done.index(k) for k in range(len(axes))]
    tiles = tiles.transpose(*back, *range(len(axes), tiles.ndim))
    return tiles.reshape(-1, *shard.shape)


def gathered_by_axis(shard, axes, sequence, dim):
    return in_order(all_blocks(shard, axes, sequence), dim)


def shifted(value, axis, steps):
    count = lax.axis_size(axis)
    first, last = (max(0, -steps), min(count, count - steps))
    return lax.ppermute(value, axis, [(source, source + steps) for source in range(first, last)])


def filled_with(shard, identity):
    return jax.tree.map(
        lambda part, zero: jnp.zeros_like(part) + jnp.asarray(zero, part.dtype), shard, identity
    )


def carried_in(shard, axes, combine, identity):
    before = start = filled_with(shard, identity)
    total = shard
    for axis in reversed(axes):
        peers, here = (lax.axis_size(axis), lax.axis_index(axis))
        pieces = jax.tree.map(
            lambda part, kind: lax.all_gather(part.astype(kind), axis),
            total,
            (jnp.bfloat16, jnp.bfloat16),
        )
        inside, total = (start, start)
        for k in range(peers):
            passed = k < here
            total = combine(
                total, jax.tree.map(lambda part, own: part[k].astype(own.dtype), pieces, shard)
            )
            inside = jax.tree.map(lambda new, old: jnp.where(passed, new, old), total, inside)
        before = combine(inside, before)
    return before


def cut_along(shard, dim, peers):
    before, after = (shard.shape[:dim], shard.shape[dim + 1 :])
    return jnp.moveaxis(shard.reshape(*before, peers, -1, *after), dim, 0)


def summed_on_arrival(shard, axis, dim):
    tiles = cut_along(shard, dim, lax.axis_size(axis))
    arrived = lax.all_to_all(tiles, axis, split_axis=0, concat_axis=0, tiled=True)
    return arrived.astype(jnp.float32).sum(axis=0)


def rms_scale(values, gain):
    return values * lax.rsqrt(jnp.mean(values * values, axis=-1, keepdims=True) + EPSILON) * gain


def join_state(earlier, later):
    decay_one, state_one = earlier
    decay_two, state_two = later
    return (decay_one * decay_two, decay_two[..., None] * state_one + state_two)


def body(
    tokens,
    input_norm_gain,
    pooling_input_weight,
    query_weight,
    forget_weight,
    value_weight,
    pooling_group_maps,
    pooling_scale,
    lower_bound_logits,
    decay_spike,
    head_norm_gain,
    pooling_output_weight,
    recurrent_output_weight,
):
    gathered = lax.all_gather(tokens, "tp", axis=1, tiled=True)[0]
    length_total = gathered.shape[0]
    normed = rms_scale(gathered.astype(jnp.float32), input_norm_gain).astype(jnp.bfloat16)
    pool_width = pooling_input_weight.shape[1]
    rec_width = query_weight.shape[1]
    stacked = jnp.concatenate(
        [pooling_input_weight, query_weight, forget_weight, value_weight], axis=1
    )
    out_local = jnp.concatenate([pooling_output_weight, recurrent_output_weight], axis=0)
    projected = jnp.dot(
        normed, lax.all_gather(stacked, SP, axis=0, tiled=True), preferred_element_type=jnp.float32
    )
    out_full = gathered_by_axis(out_local, SP, (0, 1), 1)
    rounded = lax.optimization_barrier(projected.astype(jnp.bfloat16))
    pool_input = rounded[:, :pool_width]
    query_matrix = rounded[:, pool_width : pool_width + rec_width].astype(jnp.float32)
    forget_gate_logit = rounded[:, pool_width + rec_width : pool_width + 2 * rec_width].astype(
        jnp.float32
    )
    value_projected = rounded[:, pool_width + 2 * rec_width :].astype(jnp.float32)
    groups_local = pooling_group_maps.shape[0]
    group_size = pooling_group_maps.shape[1]
    reach_rows = 2 ** (groups_local * lax.axis_size("tp"))
    previous = shifted(pool_input[length_total - reach_rows :], SP, 1)
    extended = jnp.concatenate([previous, pool_input], axis=0).astype(jnp.float32)
    extended = extended.reshape(reach_rows + length_total, groups_local, group_size)
    group_ids = lax.axis_index("tp") * groups_local + jnp.arange(groups_local, dtype=jnp.int32)
    windows = jnp.left_shift(jnp.int32(2), group_ids)
    window_sum = jnp.zeros((length_total, groups_local, group_size), jnp.float32)
    for offset in range(reach_rows):
        inside = (offset < windows).astype(jnp.float32)
        window_sum = (
            window_sum
            + extended[reach_rows - offset : reach_rows - offset + length_total] * inside[:, None]
        )
    position_index = lax.axis_index(SP) * length_total + jnp.arange(length_total, dtype=jnp.int32)
    counts = jnp.minimum(position_index[:, None] + 1, windows[None, :]).astype(jnp.float32)
    pool_diff = (window_sum / counts[:, :, None] - extended[reach_rows:]).astype(jnp.bfloat16)
    pool_mapped = jnp.einsum(
        "tgc,gcd->tgd", pool_diff, pooling_group_maps, preferred_element_type=jnp.float32
    )
    pool_out = (pool_mapped.reshape(length_total, pool_width) * pooling_scale).astype(jnp.bfloat16)
    local_heads = decay_spike.shape[2]
    head_width = rec_width // local_heads
    blocks = length_total // BLOCK
    block_layout = (blocks, BLOCK, local_heads, head_width)
    reader = jax.nn.silu(query_matrix).reshape(block_layout)
    key_gate_value = jax.nn.sigmoid(-lower_bound_logits) * jax.nn.sigmoid(-forget_gate_logit)
    decay_logarithm = (
        jnp.log1p(-key_gate_value).reshape(length_total, local_heads, head_width)
        + decay_spike[0][:, :, None]
    ).reshape(block_layout)
    key_rows = key_gate_value.reshape(block_layout)
    value_rows = value_projected.reshape(block_layout)
    inner_log = jnp.cumsum(decay_logarithm, axis=1)
    read_scaled = reader * jnp.exp(inner_log)
    key_scaled = key_rows * jnp.exp(-inner_log)
    causal = (jnp.arange(BLOCK)[:, None] >= jnp.arange(BLOCK)[None, :]).astype(jnp.float32)
    scores = jnp.einsum("nthd,nshd->nhts", read_scaled, key_scaled, precision=HIGHEST) * causal
    within = jnp.einsum("nhts,nshe->nthe", scores, value_rows, precision=HIGHEST)
    closing = inner_log[:, -1]
    key_tail = key_rows * jnp.exp(closing[:, None] - inner_log)
    deltas = jnp.einsum("nshd,nshe->nhde", key_tail, value_rows, precision=HIGHEST)
    block_decay = jnp.exp(closing)

    def advance(carried, input_batch):
        decay_now, delta_now = input_batch
        return (decay_now[..., None] * carried + delta_now, carried)

    initial = jnp.zeros((local_heads, head_width, head_width), jnp.float32)
    device_state, entry_states = lax.scan(advance, initial, (block_decay, deltas))
    device_decay = jnp.exp(jnp.sum(closing, axis=0))
    scanned = carried_in(
        (device_decay, device_state),
        SP,
        join_state,
        (jnp.ones_like(device_decay), jnp.zeros_like(device_state)),
    )
    prior_state = scanned[1]
    before = jnp.cumsum(closing, axis=0) - closing
    start_states = entry_states + jnp.exp(before)[..., None] * prior_state[None]
    read_out = within + jnp.einsum("nthd,nhde->nthe", read_scaled, start_states, precision=HIGHEST)
    read_out = read_out.reshape(length_total, local_heads, head_width)
    recurrent_output = (
        rms_scale(read_out, 1.0).reshape(length_total, rec_width) * head_norm_gain
    ).astype(jnp.bfloat16)
    mixed_rows = jnp.concatenate([pool_out, recurrent_output], axis=1)
    summed = summed_on_arrival(
        jnp.dot(mixed_rows, out_full, preferred_element_type=jnp.float32).astype(jnp.bfloat16),
        "tp",
        0,
    )
    return summed.astype(jnp.bfloat16)[None]


def solution(mesh):
    torus = Mesh(
        mesh.devices.reshape(8, 8, mesh.shape["fs"], mesh.shape["tp"]), ("sp_0", "sp_1", "fs", "tp")
    )
    return jax.shard_map(
        body,
        mesh=torus,
        in_specs=(
            P("fs", SP_TP, None),
            P(),
            P(SP, "tp"),
            P(SP, "tp"),
            P(SP, "tp"),
            P(SP, "tp"),
            P("tp", None, None),
            P("tp"),
            P("tp"),
            P("fs", SP, "tp"),
            P("tp"),
            P("tp", SP),
            P("tp", SP),
        ),
        out_specs=P("fs", SP_TP, None),
        check_vma=False,
    )
```

profile of v0, /device:TPU:1, one launch (start us, length us, event | category | flops | bytes accessed | tf_op | source)
XLA Modules:
  0.0 277.8 jit_solution(2328554561795465922)
XLA Ops:
  6.5 0.0 copy-start
  6.5 0.0 all-gather.10.cloned.1.call-start
  6.5 1.5 pad_maximum_fusion
  8.1 0.0 all-gather.10.cloned.1.call-update
  8.1 0.0 all-gather.16.cloned.1.call-start
  8.1 0.8 pad_maximum_fusion.1
  8.9 27.3 %all-gather.2 = bf16[8192,32]{0,1:T(8,128)(2,1)S(1)} all-gather(bf16[1024,32]{0,1:T(8,128)(2,1)S(1)} %pad_maximum_fusion.1), channel_id=4, replica_groups=mesh['sp_0'=8,'sp_1'=8,'fs'=4,'tp'=2] {'sp_0'}, dimensions={0}, use_global_device_ids=true | all-gather | bytes 589824 | tf_op jit(solution)/shard_map/all_gather | solution.py:25
  36.2 1.1 copy.197
  37.4 0.0 all-gather.16.cloned.1.call-update
  37.4 0.0 all-gather.14.cloned.1.call-start
  37.5 0.8 copy.177
  38.3 7.8 %all_gather.36 = bf16[1,128,2048]{2,1,0:T(8,128)(2,1)S(1)} all-gather(bf16[1,64,2048]{2,1,0:T(8,128)(2,1)} %param.15), channel_id=1, replica_groups=mesh['sp_0'=8,'sp_1'=8,'fs'=4,'tp'=2] {'tp'}, dimensions={1}, use_global_device_ids=true | all-gather | bytes 786432 | tf_op jit(solution)/shard_map/all_gather | solution.py:105
  46.2 0.2 fusion.2
  46.4 0.7 add_divide_fusion
  47.0 67.8 %all-gather.10.cloned.1.call-done = bf16[2048,2048]{1,0:T(8,128)(2,1)} async-done(((bf16[32,2048]{1,0:T(8,128)(2,1)}), bf16[2048,2048]{1,0:T(8,128)(2,1)}) %all-gather.10.cloned.1.call-update) | async-done | bytes 8388624 | tf_op jit(solution)/shard_map/all_gather | solution.py:115
  114.9 4.7 %convolution_convert_fusion = bf16[128,2048]{1,0:T(8,128)(2,1)S(1)} fusion(bf16[2048,2048]{1,0:T(8,128)(2,1)} %all-gather.10.cloned.1.call-done, bf16[1,128,2048]{2,1,0:T(8,128)(2,1)S(1)} %all_gather.36, f32[2048]{0:T(1024)} %param.16, f32[128]{0:T(128)S(1)} %add_rsqrt_fusion.1), kind=kOutput, calls=%fused_computation.3 | convolution fusion | flops 1075052544 | bytes 9445888 | tf_op jit(solution)/shard_map/dot_general | solution.py:114
  119.6 0.2 negate_log-plus-one_fusion
  119.8 0.1 reshape.384
  119.9 0.1 reshape.383
  120.0 0.1 reshape.385
  120.2 0.2 fusion.54
  120.4 0.2 exponential_multiply_fusion
  120.6 0.6 fusion.48
  121.2 0.5 while.13
  121.3 0.2 bitcast_add_fusion.2
  121.5 0.2 bitcast_add_fusion.2
  121.7 0.7 convert_element_type.533
  122.4 0.0 all-gather.14.cloned.1.call-update
  122.4 0.0 all-gather.12.cloned.1.call-start
  122.6 0.1 minimum_convert_fusion
  122.7 49.5 %all-gather.16.cloned.1.call-done = bf16[64,1024,32]{1,0,2:T(8,128)(2,1)} async-done(((bf16[8,1024,32]{1,0,2:T(8,128)(2,1)}), bf16[64,1024,32]{1,0,2:T(8,128)(2,1)}) %all-gather.16.cloned.1.call-update) | async-done | bytes 4194320 | tf_op jit(solution)/shard_map/all_gather | solution.py:25
  172.2 6.5 %copy.176 = bf16[8,8,1024,32]{2,3,1,0:T(8,128)(2,1)} copy(bf16[8,8,1024,32]{2,0,1,3:T(8,128)(2,1)} %bitcast.379) | data formatting | bytes 8388608 | tf_op jit(solution)/shard_map/transpose | solution.py:28
  178.7 11.0 %all-gather.4 = bf16[8,4,128]{2,1,0:T(4,128)(2,1)S(1)} all-gather(bf16[1,4,128]{2,1,0:T(4,128)(2,1)S(1)} %fusion.75), channel_id=2, replica_groups=mesh['sp_0'=8,'sp_1'=8,'fs'=4,'tp'=2] {'sp_1'}, dimensions={0}, use_global_device_ids=true | all-gather | bytes 9216 | tf_op jit(solution)/shard_map/all_gather | solution.py:54
  189.6 14.1 %all_gather.39 = bf16[8,4,128]{2,1,0:T(4,128)(2,1)S(1)} all-gather(bf16[1,4,128]{2,1,0:T(4,128)(2,1)S(1)} %fusion.65), channel_id=1, replica_groups=mesh['sp_0'=8,'sp_1'=8,'fs'=4,'tp'=2] {'sp_0'}, dimensions={0}, use_global_device_ids=true | all-gather | bytes 9216 | tf_op jit(solution)/shard_map/all_gather | solution.py:54
  203.8 5.7 %all-gather.14.cloned.1.call-done = bf16[32,128,128]{2,1,0:T(8,128)(2,1)} async-done(((bf16[4,128,128]{2,1,0:T(8,128)(2,1)}), bf16[32,128,128]{2,1,0:T(8,128)(2,1)}) %all-gather.14.cloned.1.call-update) | async-done | bytes 1048592 | tf_op jit(solution)/shard_map/all_gather | solution.py:54
  209.4 2.4 fusion.52
  211.9 0.0 all-gather.12.cloned.1.call-update
  211.9 2.7 collective-permute-start
  214.6 0.5 convolution_multiply_fusion
  215.2 0.3 fusion.62
  215.4 0.0 collective-permute-done
  215.5 0.5 fusion.90
  216.0 0.0 copy-start.2
  216.0 0.0 copy-start.1
  216.0 0.0 copy-done
  216.0 0.5 convolution_bitcast_fusion
  216.5 0.0 copy-start.3
  216.5 0.1 copy.164
  216.7 0.0 copy-done.2
  216.7 0.1 fusion.47
  216.8 36.3 %all-gather.12.cloned.1.call-done = bf16[8,4,128,128]{3,2,1,0:T(8,128)(2,1)} async-done(((bf16[1,4,128,128]{3,2,1,0:T(8,128)(2,1)}), bf16[8,4,128,128]{3,2,1,0:T(8,128)(2,1)}) %all-gather.12.cloned.1.call-update) | async-done | bytes 1048592 | tf_op jit(solution)/shard_map/all_gather | solution.py:54
  253.1 0.0 copy-done.1
  253.1 2.9 %fusion.44 = f32[4,128,128]{2,1,0:T(8,128)S(1)} fusion(bf16[8,4,128,128]{3,2,1,0:T(8,128)(2,1)} %all-gather.12.cloned.1.call-done, f32[4,128]{1,0:T(4,128)S(1)} %get-tuple-element.90, f32[4,128]{1,0:T(4,128)S(1)} %get-tuple-element.104, f32[4,128]{1,0:T(4,128)S(1)} %get-tuple-element.103, f32[4,128]{1,0:T(4,128)S(1)} %get-tuple-element.102, ...), kind=kLoop, calls=%fused_computation.80 | loop fusion | flops 4194304 | bytes 2394128 | tf_op jit(solution)/shard_map/mul | solution.py:185
  256.1 0.8 multiply_reduce_fusion
  256.9 0.3 copy.178
  257.1 0.3 reshape.475
  257.4 0.1 rsqrt.21
  257.5 0.0 copy-done.3
  257.5 0.1 fusion.46
  257.7 3.7 %convolution_convert_fusion.1 = bf16[128,2048]{1,0:T(8,128)(2,1)S(1)} fusion(bf16[1024,2048]{0,1:T(8,128)(2,1)} %bitcast.378, bf16[128,512]{0,1:T(8,128)(2,1)S(1)} %fusion.46, bf16[128,512]{0,1:T(8,128)(2,1)S(1)} %fusion.47), kind=kOutput, calls=%fused_computation.4 | convolution fusion | flops 537657344 | bytes 4980736 | tf_op jit(solution)/shard_map/dot_general | solution.py:193
  261.4 9.1 %all_to_all.5 = bf16[2,64,2048]{2,1,0:T(8,128)(2,1)S(1)} all-to-all(bf16[2,64,2048]{2,1,0:T(8,128)(2,1)S(1)} %bitcast.380), channel_id=1, replica_groups=mesh['sp_0'=8,'sp_1'=8,'fs'=4,'tp'=2] {'tp'}, dimensions={0} | all-to-all | bytes 1048576 | tf_op jit(solution)/shard_map/all_to_all | solution.py:76
  270.5 0.8 reduce_sum.42
  (33 shorter events, 0.3 us)
Async XLA Ops:
  6.5 209.5 %copy-start = (bf16[2,256,256]{2,1,0:T(8,128)(2,1)S(1)}, bf16[2,256,256]{2,1,0:T(8,128)(2,1)}, u32[]{:S(2)}) copy-start(bf16[2,256,256]{2,1,0:T(8,128)(2,1)} %param.21) | copy-start | bytes 786436
  6.5 108.3 %all-gather.10.cloned.1.call-start = ((), (), s32[]{:S(2)}) async-start(), calls=%async_computation.1 | async-start | bytes 8519680 | tf_op jit(solution)/shard_map/all_gather | solution.py:115
  8.1 164.1 %all-gather.16.cloned.1.call-start = ((), (), s32[]{:S(2)}) async-start(), calls=%async_computation.4 | async-start | bytes 4718592 | tf_op jit(solution)/shard_map/all_gather | solution.py:25
  37.4 172.1 %all-gather.14.cloned.1.call-start = ((), (), s32[]{:S(2)}) async-start(), calls=%async_computation.3 | async-start | bytes 1179648 | tf_op jit(solution)/shard_map/all_gather | solution.py:54
  122.4 130.7 %all-gather.12.cloned.1.call-start = ((), (), s32[]{:S(2)}) async-start(), calls=%async_computation.2 | async-start | bytes 1179648 | tf_op jit(solution)/shard_map/all_gather | solution.py:54
  211.9 3.5 %collective-permute-start = (bf16[16,512]{1,0:T(8,128)(2,1)S(1)}, bf16[16,512]{1,0:T(8,128)(2,1)S(1)}, u32[]{:S(2)}, u32[]{:S(2)}) collective-permute-start(bf16[16,512]{1,0:T(8,128)(2,1)S(1)} %slice.306), channel_id=1, source_target_pairs={{0,8},{8,16},{16,24},{24,32},{32,40},{40,48},{48,56},{56,64},{64,7... | collective-permute-start | bytes 49160 | tf_op jit(solution)/shard_map/ppermute | solution.py:39
  216.0 0.7 copy-start.2
  216.0 37.1 %copy-start.1 = (bf16[32,128,128]{2,1,0:T(8,128)(2,1)S(1)}, bf16[32,128,128]{2,1,0:T(8,128)(2,1)}, u32[]{:S(2)}) copy-start(bf16[32,128,128]{2,1,0:T(8,128)(2,1)} %all-gather.14.cloned.1.call-done) | copy-start | bytes 3145732
  216.5 41.0 %copy-start.3 = (f32[512]{0:T(512)S(1)}, f32[512]{0:T(512)}, u32[]{:S(2)}) copy-start(f32[512]{0:T(512)} %param.25) | copy-start | bytes 6148
Sparse Core Ops, SparseCore 0:
  10.4 104.4 all-gather.9
  117.0 55.1 all-gather.15
  174.3 35.1 all-gather.13
  212.0 41.0 all-gather.11
where the time goes:
time: 279 us; the launch traced here: 278 us
  waiting for transfers between devices  159 us (57%)
  blocking collectives  69.3 us (25%)
  between operations  13.5 us (5%)
  other arithmetic  11.6 us (4%)
  matrix products  11.1 us (4%)
  local copies, waits for them, and re-layouts  10 us (4%)
  starting transfers between devices  2.81 us (1%)
    all_gather x1, waiting for transfers between devices, body(): lax.all_gather(stacked, SP, axis=0, tiled=True)  67.8 us
    all_gather x1, waiting for transfers between devices, all_blocks(): tiles = lax.all_gather(tiles, axes[k])  49.5 us
    all_gather x2, waiting for transfers between devices, carried_in(): lax.all_gather(part.astype(kind), axis)  42 us
    all_gather x1, blocking collectives, all_blocks(): tiles = lax.all_gather(tiles, axes[k])  27.3 us
    all_gather x2, blocking collectives, carried_in(): lax.all_gather(part.astype(kind), axis)  25.1 us
    all_to_all x1, blocking collectives, summed_on_arrival(): lax.all_to_all(tiles, axis, split_axis=0, concat_axis=0, tiled=True)  9.09 us
    all_gather x1, blocking collectives, body(): gathered = lax.all_gather(tokens, 'tp', axis=1, tiled=True)[0]  7.83 us
    transpose x1, local copies, waits for them, and re-layouts, all_blocks(): tiles = tiles.transpose(*back, *range(len(axes), tiles.ndim))  6.47 us
  transfers between devices with their start and end apart: 5, of which 4 were waited for; matrix products, arithmetic and copies ran while one was open for 7% of the time, Pallas kernels for 0%

commit v1 on v0

v1 whole, which is shorter than its diff:
```python
import functools

import jax
import jax.numpy as jnp
from jax import lax
from jax.experimental import pallas as pl
from jax.experimental.pallas import tpu as pltpu
from jax.sharding import Mesh
from jax.sharding import PartitionSpec as P

MESH = pl.DeviceIdType.MESH
BLOCK = 64
HEAD = 128
TOK = 128
HALF = 64
WROWS = 16
WCOLS = 256
HALO = 16
EPS = 1e-06
F32 = jnp.float32
BF16 = jnp.bfloat16


def three_parts(value):
    high = value.astype(BF16)
    rest = value - high.astype(F32)
    mid = rest.astype(BF16)
    low = (rest - mid.astype(F32)).astype(BF16)
    return high, mid, low


def nt(a, b):
    return lax.dot_general(a, b, (((1,), (1,)), ((), ())), preferred_element_type=F32)


def tn(a, b):
    return lax.dot_general(a, b, (((0,), (0,)), ((), ())), preferred_element_type=F32)


def nn(a, b):
    return jnp.dot(a, b, preferred_element_type=F32)


def kernel(
    sizes,
    tok_ref,
    gin_ref,
    wp_ref,
    wq_ref,
    wf_ref,
    wv_ref,
    maps_ref,
    scale_ref,
    lb_ref,
    spike_ref,
    hg_ref,
    wpo_ref,
    wro_ref,
    out_ref,
    tokbuf,
    wbuf,
    wobuf,
    wop,
    wor,
    spbuf,
    fbuf,
    vbuf,
    qbuf,
    pbuf,
    cfull,
    inner_buf,
    c1_send,
    c1_recv,
    pex,
    dex,
    c2_send,
    c2_recv,
    c3_send,
    c3_recv,
    halo,
    within,
    xpool,
    xrec,
    pacc,
    parts,
    part_in,
    mixed,
    obuf,
    p1_ss,
    p1_rs,
    p2_ss,
    p2_rs,
    tok_ss,
    tok_rs,
    d2d_ss,
    d2d_rs,
    sp_ss,
    sp_rs,
    c1_ss,
    c1_rs,
    c2_ss,
    c2_rs,
    c3_ss,
    c3_rs,
    halo_ss,
    halo_rs,
    xp_ss,
    xp_rs,
    xr_ss,
    xr_rs,
    part_ss,
    part_rs,
    o_ss,
    o_rs,
):
    nz, ny, nx = sizes
    z, y, x, c = (lax.axis_index(name) for name in ("z", "y", "x", "c"))
    sp = z * ny + y
    width = tok_ref.shape[2]
    wo_cols = 32 // nx
    piece = HEAD // ny
    packed = nx * piece
    half_pool = nx * HEAD

    def rc(src, dst, ss, rs, **device):
        return pltpu.make_async_remote_copy(
            src_ref=src, dst_ref=dst, send_sem=ss, recv_sem=rs, device_id=device, device_id_type=MESH
        )

    def at(base, step, count):
        return lax.rem(base + step + count, count)

    barrier = pltpu.get_barrier_semaphore()

    def greet(**device):
        pl.semaphore_signal(barrier, inc=1, device_id=device, device_id_type=MESH)

    for k in range(1, ny):
        greet(y=at(y, k, ny))
    for k in range(1, nz):
        greet(z=at(z, k, nz))
    for k in range(1, nx):
        greet(x=at(x, k, nx))
    greet(c=1 - c)
    if nz > 1 and ny > 1:
        down = jnp.logical_and(y == ny - 1, z < nz - 1)
        up = jnp.logical_and(y == 0, z > 0)

        @pl.when(down)
        def _():
            greet(z=z + 1, y=0)

        @pl.when(up)
        def _():
            greet(z=z - 1, y=ny - 1)

    own = tok_ref[0].astype(F32)
    square = jnp.mean(own * own, axis=-1, keepdims=True)
    tokbuf[x, c] = (own * lax.rsqrt(square + EPS) * gin_ref[...]).astype(BF16)
    lanes = pl.ds(pl.multiple_of(x * HEAD, HEAD), HEAD)
    for p in range(2):
        rows = slice(p * WROWS, (p + 1) * WROWS)
        wbuf[0, z, y, p, :, 0:HEAD] = wf_ref[rows, lanes]
        wbuf[0, z, y, p, :, HEAD:WCOLS] = wv_ref[rows, lanes]
        wbuf[1, z, y, p, :, 0:HEAD] = wp_ref[rows, lanes]
        wbuf[1, z, y, p, :, HEAD:WCOLS] = wq_ref[rows, lanes]
    heads = spike_ref.shape[2]
    pick = (
        lax.broadcasted_iota(jnp.int32, (8, heads), 0)
        == lax.broadcasted_iota(jnp.int32, (8, heads), 1)
    ).astype(F32)
    spbuf[x] = lax.dot_general(
        pick,
        spike_ref[0],
        (((1,), (1,)), ((), ())),
        precision=lax.Precision.HIGHEST,
        preferred_element_type=F32,
    )

    greeted = (ny - 1) + (nz - 1) + (nx - 1) + 1
    if nz > 1 and ny > 1:
        at_end = (y // (ny - 1)) * (1 - z // (nz - 1))
        at_start = ((ny - 1 - y) // (ny - 1)) * (1 - (nz - 1 - z) // (nz - 1))
        greeted = greeted + at_end + at_start
    pl.semaphore_wait(barrier, greeted)

    def p1(st, k, path):
        if path == 0:
            return lambda zz, zt: rc(
                wbuf.at[st, zz, y, 0],
                wbuf.at[st, zz, y, 0],
                p1_ss.at[st, 0, k - 1],
                p1_rs.at[st, 0, k - 1],
                z=zt,
            )
        return lambda yy, yt: rc(
            wbuf.at[st, z, yy, 1],
            wbuf.at[st, z, yy, 1],
            p1_ss.at[st, 1, k - 1],
            p1_rs.at[st, 1, k - 1],
            y=yt,
        )

    def p1_send(st):
        for k in range(1, max(nz, ny)):
            if k < nz:
                p1(st, k, 0)(z, at(z, k, nz)).start()
            if k < ny:
                p1(st, k, 1)(y, at(y, k, ny)).start()

    def p1_wait(st):
        for k in range(1, nz):
            p1(st, k, 0)(at(z, -k, nz), at(z, -k, nz)).wait_recv()
        for k in range(1, ny):
            p1(st, k, 1)(at(y, -k, ny), at(y, -k, ny)).wait_recv()

    def p1_done(st):
        for k in range(1, nz):
            p1(st, k, 0)(z, at(z, k, nz)).wait_send()
        for k in range(1, ny):
            p1(st, k, 1)(y, at(y, k, ny)).wait_send()

    routes = []
    for path, count in ((0, ny), (1, nz)):
        for way in range(2):
            routes.append((path, way, count // 2 if way == 0 else (count - 1) // 2))

    def p2(st, path, way, step, distance, to):
        sign = 1 if way == 0 else -1
        if path == 0:
            block = wbuf.at[st, :, at(y, -sign * distance, ny), 0]
            device = {"y": at(y, sign * to, ny)}
        else:
            block = wbuf.at[st, at(z, -sign * distance, nz), :, 1]
            device = {"z": at(z, sign * to, nz)}
        return rc(
            block, block, p2_ss.at[st, path, way, step], p2_rs.at[st, path, way, step], **device
        )

    steps = max(r[2] for r in routes)

    def p2_send(st, step):
        for path, way, count in routes:
            if step < count:
                p2(st, path, way, step, step, 1).start()

    def p2_wait(st, step):
        for path, way, count in routes:
            if step < count:
                p2(st, path, way, step, step + 1, 1).wait_recv()

    def p2_advance(st, step):
        for path, way, count in routes:
            if step - 1 < count:
                p2(st, path, way, step - 1, step, 1).wait_recv()
            if step < count:
                p2(st, path, way, step, step, 1).start()

    def p2_done(st):
        for path, way, count in routes:
            for step in range(count):
                p2(st, path, way, step, step, 1).wait_send()

    right, left, across = at(x, 1, nx), at(x, -1, nx), at(x, 2, nx)

    def ring_x(part, ss, rs):
        def move(slot, owner, half, to):
            return rc(part(owner, half), part(owner, half), ss.at[slot], rs.at[slot], x=to)

        class Ring:
            def start_first(self):
                move(0, x, 0, right).start()
                move(2, x, 1, left).start()

            def start_second(self):
                move(1, x, 1, right).start()
                move(3, x, 0, left).start()

            def start(self):
                self.start_first()
                self.start_second()

            def forward(self):
                move(0, left, 0, right).wait_recv()
                move(4, left, 0, right).start()
                move(2, right, 1, left).wait_recv()
                move(5, right, 1, left).start()

            def near(self):
                move(1, left, 1, right).wait_recv()
                move(3, right, 0, left).wait_recv()

            def far(self):
                move(4, across, 0, right).wait_recv()
                move(5, across, 1, left).wait_recv()

            def done(self):
                for slot, owner, half, to in (
                    (0, x, 0, right),
                    (1, x, 1, right),
                    (2, x, 1, left),
                    (3, x, 0, left),
                    (4, left, 0, right),
                    (5, right, 1, left),
                ):
                    move(slot, owner, half, to).wait_send()

        return Ring()

    tokens = ring_x(
        lambda owner, half: tokbuf.at[owner, c, pl.ds(half * (HALF // 2), HALF // 2)], tok_ss, tok_rs
    )

    def to_partner(slot, owner, core):
        return rc(
            tokbuf.at[owner, core], tokbuf.at[owner, core], d2d_ss.at[slot], d2d_rs.at[slot], c=1 - c
        )

    def spikes(k, owner):
        return rc(spbuf.at[owner], spbuf.at[owner], sp_ss.at[k - 1], sp_rs.at[k - 1], x=at(x, k, nx))

    p1_send(0)
    tokens.start()
    to_partner(0, x, c).start()
    for k in range(1, nx):
        spikes(k, x).start()
    p1_send(1)

    wobuf[0] = wpo_ref[...].astype(F32).T
    wobuf[1] = wro_ref[...].astype(F32).T
    mine = pl.ds(pl.multiple_of(x * wo_cols, wo_cols), wo_cols)
    block = jnp.concatenate([wobuf[0, mine, :], wobuf[1, mine, :]], axis=0).astype(BF16)
    for p in range(2):
        wbuf[2, z, y, p] = block[:, p * WCOLS : (p + 1) * WCOLS]

    p1_wait(0)
    p2_send(0, 0)
    tokens.forward()
    p1_wait(1)
    p2_send(1, 0)
    tokens.near()
    to_partner(1, left, c).start()
    to_partner(2, right, c).start()
    p1_send(2)
    for step in range(1, steps):
        p2_advance(0, step)
        p2_advance(1, step)
        if step == 1:
            tokens.far()
            to_partner(3, across, c).start()
    for slot, owner in enumerate((x, left, right, across)):
        to_partner(slot, owner, 1 - c).wait_recv()
    for k in range(1, nx):
        spikes(k, at(x, -k, nx)).wait_recv()
    p2_wait(0, steps - 1)

    rows = nx * TOK

    def project(st):
        return nn(tokbuf[...].reshape(rows, width), wbuf[st].reshape(width, WCOLS)).astype(BF16)

    projected = project(0)
    fbuf[...] = projected[:, :HEAD]
    vbuf[...] = projected[:, HEAD:]

    ti = lax.broadcasted_iota(jnp.int32, (TOK, TOK), 0)
    si = lax.broadcasted_iota(jnp.int32, (TOK, TOK), 1)
    same = (ti // BLOCK) == (si // BLOCK)
    causal = jnp.logical_and(same, ti >= si)
    lower = causal.astype(F32)
    lower_b = lower.astype(BF16)
    ones_b = jnp.ones((TOK, HEAD), BF16)
    second = lax.broadcasted_iota(jnp.int32, (TOK, HEAD), 0) >= BLOCK
    lb_gate = 1.0 / (1.0 + jnp.exp(lb_ref[pl.ds(x, 1), :]))
    decays = []
    for s in range(nx):
        span = slice(s * TOK, (s + 1) * TOK)
        key = lb_gate * (1.0 / (1.0 + jnp.exp(fbuf[span, :].astype(F32))))
        logs = three_parts(jnp.log1p(-key))
        spike_row = spbuf[s, pl.ds(x, 1), :]
        spread = three_parts(lower * spike_row)
        inner = nn(
            jnp.concatenate([lower_b, lower_b, lower_b, *spread], axis=1),
            jnp.concatenate([*logs, ones_b, ones_b, ones_b], axis=0),
        )
        first_end = inner[BLOCK - 1 : BLOCK, :]
        total = first_end + inner[TOK - 1 : TOK, :]
        full = inner + jnp.where(second, first_end, 0.0)
        inner_buf[span, :] = inner
        cfull[span, :] = full
        tail = (key * jnp.exp(total - full)).astype(BF16)
        state = tn(vbuf[span, :], tail).astype(BF16)
        for j in range(ny):
            c1_send[j, s * piece : (s + 1) * piece, :] = state[j * piece : (j + 1) * piece, :]
        decays.append(jnp.exp(total))

    def decay_rows(values):
        out = []
        for value in values:
            high = value.astype(BF16).astype(F32)
            out += [high, value - high]
        out.append(jnp.zeros((16 - len(out), HEAD), F32))
        return jnp.concatenate(out, axis=0).astype(BF16)

    extra = decay_rows(decays)
    for j in range(ny):
        c1_send[j, packed : packed + 16, :] = extra
    c1_recv[y] = c1_send[y]

    def c1(k, slot):
        to = at(y, k, ny)
        return rc(c1_send.at[to], c1_recv.at[slot], c1_ss.at[k - 1], c1_rs.at[k - 1], y=to)

    for k in range(1, ny):
        c1(k, y).start()

    p1_wait(2)
    p2_wait(1, steps - 1)
    p2_send(2, 0)
    projected = project(1)
    pbuf[...] = projected[:, :HEAD].reshape(nx, TOK, HEAD)
    qbuf[...] = projected[:, HEAD:]

    last = nz * ny - 1
    halo_src = pbuf.at[:, TOK - HALO : TOK]

    def halo_copy(**device):
        return rc(halo_src, halo, halo_ss, halo_rs, **device)

    if ny > 1:

        @pl.when(y < ny - 1)
        def _():
            halo_copy(y=y + 1).start()

    if nz > 1:

        @pl.when(jnp.logical_and(y == ny - 1, z < nz - 1))
        def _():
            halo_copy(z=z + 1, y=0).start()

    @pl.when(sp == 0)
    def _():
        halo[...] = jnp.zeros_like(halo)

    for k in range(1, ny):
        c1(k, at(y, -k, ny)).wait_recv()

    def read_decay(block, s):
        at_row = packed + 2 * s
        return block[at_row : at_row + 1, :] + block[at_row + 1 : at_row + 2, :]

    run = [jnp.zeros((piece, HEAD), F32) for _ in range(nx)]
    fade = [jnp.ones((1, HEAD), F32) for _ in range(nx)]
    for j in range(ny):
        block = c1_recv[j].astype(F32)
        for s in range(nx):
            pex[j, s * piece : (s + 1) * piece, :] = run[s]
            dex[j, s : s + 1, :] = fade[s]
            decay = read_decay(block, s)
            run[s] = decay * run[s] + block[s * piece : (s + 1) * piece, :]
            fade[s] = fade[s] * decay
    c2_send[0:packed, :] = jnp.concatenate(run, axis=0).astype(BF16)
    c2_send[packed : packed + 16, :] = decay_rows(fade)

    def c2(k, slot, to):
        return rc(c2_send, c2_recv.at[slot], c2_ss.at[k - 1], c2_rs.at[k - 1], z=to)

    if nz > 1:

        def send_later(k, _):
            c2(k, z, z + k).start()
            return _

        lax.fori_loop(1, nz - z, send_later, 0)

    for s in range(nx):
        span = slice(s * TOK, (s + 1) * TOK)
        query = qbuf[span, :].astype(F32)
        reader = query * (1.0 / (1.0 + jnp.exp(-query)))
        key = lb_gate * (1.0 / (1.0 + jnp.exp(fbuf[span, :].astype(F32))))
        inner = inner_buf[span, :]
        scaled = (reader * jnp.exp(inner)).astype(BF16)
        near = (key * jnp.exp(-inner)).astype(BF16)
        tail = (
            key[:BLOCK] * jnp.exp(inner[BLOCK - 1 : BLOCK, :] - inner[:BLOCK])
        ).astype(BF16)
        scores = nt(scaled, jnp.concatenate([near, tail], axis=0))
        cross = jnp.concatenate([scores[:, TOK:], scores[:, TOK:]], axis=1)
        before = jnp.logical_and(ti >= BLOCK, si < BLOCK)
        chosen = jnp.where(causal, scores[:, :TOK], jnp.where(before, cross, 0.0))
        within[span, :] = nn(chosen.astype(BF16), vbuf[span, :])
        cfull[span, :] = reader * jnp.exp(cfull[span, :])
    if steps > 1:
        p2_advance(2, 1)

    if ny > 1:

        @pl.when(y > 0)
        def _():
            halo_copy(y=y - 1).wait_recv()

    if nz > 1:

        @pl.when(jnp.logical_and(y == 0, z > 0))
        def _():
            halo_copy(z=z - 1, y=ny - 1).wait_recv()

    group = (c * half_pool + x * HEAD) // WCOLS
    window = jnp.where(group == 0, 2, jnp.where(group == 1, 4, jnp.where(group == 2, 8, 16)))
    band = jnp.logical_and(ti >= si, ti - si < window).astype(BF16)
    hi = lax.broadcasted_iota(jnp.int32, (TOK, HALO), 0)
    hj = lax.broadcasted_iota(jnp.int32, (TOK, HALO), 1)
    band_before = (hi + HALO - hj < window).astype(BF16)
    place = sp * TOK + lax.broadcasted_iota(jnp.int32, (TOK, HEAD), 0) + 1
    count = jnp.minimum(place, window).astype(F32)
    for s in range(nx):
        sums = nn(band, pbuf[s]) + nn(band_before, halo[s])
        xpool[x, s * TOK : (s + 1) * TOK, :] = (sums / count - pbuf[s].astype(F32)).astype(BF16)

    half_rows = rows // 2
    pool_ring = ring_x(
        lambda owner, half: xpool.at[owner, pl.ds(half * half_rows, half_rows)], xp_ss, xp_rs
    )
    rec_ring = ring_x(
        lambda owner, half: xrec.at[owner, pl.ds(half * half_rows, half_rows)], xr_ss, xr_rs
    )
    pool_ring.start()

    def add_row(zz, carry):
        if nz > 1:
            rc(
                c2_send, c2_recv.at[zz], c2_ss.at[z - zz - 1], c2_rs.at[z - zz - 1], z=zz
            ).wait_recv()
        block = c2_recv[zz].astype(F32)
        out = []
        for s in range(nx):
            out.append(
                read_decay(block, s) * carry[s] + block[s * piece : (s + 1) * piece, :]
            )
        return tuple(out)

    earlier = tuple(jnp.zeros((piece, HEAD), F32) for _ in range(nx))
    if nz > 1:
        earlier = lax.fori_loop(0, z, add_row, earlier)
    for j in range(ny):
        for s in range(nx):
            span = slice(s * piece, (s + 1) * piece)
            c3_send[j, span, :] = (dex[j, s : s + 1, :] * earlier[s] + pex[j, span, :]).astype(BF16)
    c3_recv[y] = c3_send[y]

    def c3(k, slot):
        to = at(y, k, ny)
        return rc(c3_send.at[to], c3_recv.at[slot], c3_ss.at[k - 1], c3_rs.at[k - 1], y=to)

    for k in range(1, ny):
        c3(k, y).start()

    pool_ring.forward()
    for step in range(2, steps):
        p2_advance(2, step)
    p2_wait(2, steps - 1)
    for p in range(2):
        both = wbuf[2, :, :, p].reshape(nz * ny, 2 * wo_cols, WCOLS).astype(F32)
        cols = slice(p * WCOLS, (p + 1) * WCOLS)
        wop[:, cols] = both[:, :wo_cols].reshape(nz * ny * wo_cols, WCOLS).astype(BF16)
        wor[:, cols] = both[:, wo_cols:].reshape(nz * ny * wo_cols, WCOLS).astype(BF16)

    for k in range(1, ny):
        c3(k, at(y, -k, ny)).wait_recv()
    gain = hg_ref[pl.ds(x, 1), :]

    def finish(s):
        span = slice(s * TOK, (s + 1) * TOK)
        prior = c3_recv[:, s * piece : (s + 1) * piece, :].reshape(HEAD, HEAD)
        read = within[span, :] + nt(cfull[span, :].astype(BF16), prior)
        square = jnp.mean(read * read, axis=-1, keepdims=True)
        xrec[x, span, :] = (read * lax.rsqrt(square + EPS) * gain).astype(BF16)

    for s in range(nx):
        finish(s)
    rec_ring.start()

    pool_ring.near()
    pool_ring.far()
    pieces = []
    for g in range(half_pool // WCOLS):
        cols = slice(g * WCOLS, (g + 1) * WCOLS)
        diff = jnp.concatenate([xpool[2 * g], xpool[2 * g + 1]], axis=1)
        pieces.append((nn(diff, maps_ref[g]) * scale_ref[:, cols]).astype(BF16))
    rec_ring.forward()
    pacc[...] = nt(jnp.concatenate(pieces, axis=1), wop[...])
    rec_ring.near()
    rec_ring.far()
    rec = jnp.concatenate([xrec[i] for i in range(nx)], axis=1)
    cols_out = nz * ny * wo_cols
    parts[...] = (
        (pacc[...] + nt(rec, wor[...])).astype(BF16).reshape(nx, 2, HALF, cols_out)
    )

    def to_half(s):
        return rc(parts.at[s, 1 - c], part_in.at[s], part_ss.at[s], part_rs.at[s], c=1 - c)

    for s in range(nx):
        to_half(s).start()

    def deliver(k, owner):
        to = at(x, k, nx)
        return rc(mixed.at[to], obuf.at[owner], o_ss.at[k - 1], o_rs.at[k - 1], x=to)

    for s in range(nx):
        to_half(s).wait_recv()
        mixed[s] = (parts[s, c].astype(F32) + part_in[s].astype(F32)).astype(BF16)
    for k in range(1, nx):
        deliver(k, x).start()
    obuf[x] = mixed[x]
    for k in range(1, nx):
        deliver(k, at(x, -k, nx)).wait_recv()

    chunk = min(HEAD, cols_out)
    total_cols = chunk * nx
    src = lax.broadcasted_iota(jnp.int32, (total_cols, total_cols), 0)
    dst = lax.broadcasted_iota(jnp.int32, (total_cols, total_cols), 1)
    wanted = (
        lax.div(lax.rem(dst, 32), wo_cols) * chunk
        + lax.div(dst, 32) * wo_cols
        + lax.rem(dst, wo_cols)
    )
    order = (src == wanted).astype(BF16)
    for q in range(cols_out // chunk):
        cols = slice(q * chunk, (q + 1) * chunk)
        joined = jnp.concatenate([obuf[i, :, cols] for i in range(nx)], axis=1)
        out_ref[0, :, q * total_cols : (q + 1) * total_cols] = nn(joined, order).astype(BF16)

    for st in range(3):
        p1_done(st)
        p2_done(st)
    tokens.done()
    pool_ring.done()
    rec_ring.done()
    for slot, owner in enumerate((x, left, right, across)):
        to_partner(slot, owner, c).wait_send()
    for k in range(1, nx):
        spikes(k, x).wait_send()
        deliver(k, x).wait_send()
    for k in range(1, ny):
        c1(k, y).wait_send()
        c3(k, y).wait_send()
    if nz > 1:

        def sent_later(k, _):
            c2(k, z, z + k).wait_send()
            return _

        lax.fori_loop(1, nz - z, sent_later, 0)
    for s in range(nx):
        to_half(s).wait_send()

    @pl.when(sp < last)
    def _():
        halo_copy(c=1 - c).wait_send()


def body(sizes, *arrays):
    nz, ny, nx = sizes
    (tok, gin, wp, wq, wf, wv, maps, scale, lb, spike, hg, wpo, wro) = arrays
    width = tok.shape[2]
    rows = nx * TOK
    piece = HEAD // ny
    packed = nx * piece
    wo_cols = 32 // nx
    cols_out = nz * ny * wo_cols
    kdim = nx * HEAD
    steps = max(ny // 2, nz // 2)
    ring = [pltpu.SemaphoreType.DMA((6,))] * 2
    scratch = [
        pltpu.VMEM((nx, 2, HALF, width), BF16),
        pltpu.VMEM((3, nz, ny, 2, WROWS, WCOLS), BF16),
        pltpu.VMEM((2, 32, kdim), F32),
        pltpu.VMEM((cols_out, kdim), BF16),
        pltpu.VMEM((cols_out, kdim), BF16),
        pltpu.VMEM((nx, 8, TOK), F32),
        pltpu.VMEM((rows, HEAD), BF16),
        pltpu.VMEM((rows, HEAD), BF16),
        pltpu.VMEM((rows, HEAD), BF16),
        pltpu.VMEM((nx, TOK, HEAD), BF16),
        pltpu.VMEM((rows, HEAD), F32),
        pltpu.VMEM((rows, HEAD), F32),
        pltpu.VMEM((ny, packed + 16, HEAD), BF16),
        pltpu.VMEM((ny, packed + 16, HEAD), BF16),
        pltpu.VMEM((ny, packed, HEAD), F32),
        pltpu.VMEM((ny, 8, HEAD), F32),
        pltpu.VMEM((packed + 16, HEAD), BF16),
        pltpu.VMEM((nz, packed + 16, HEAD), BF16),
        pltpu.VMEM((ny, packed, HEAD), BF16),
        pltpu.VMEM((ny, packed, HEAD), BF16),
        pltpu.VMEM((nx, HALO, HEAD), BF16),
        pltpu.VMEM((rows, HEAD), F32),
        pltpu.VMEM((nx, rows, HEAD), BF16),
        pltpu.VMEM((nx, rows, HEAD), BF16),
        pltpu.VMEM((rows, cols_out), F32),
        pltpu.VMEM((nx, 2, HALF, cols_out), BF16),
        pltpu.VMEM((nx, HALF, cols_out), BF16),
        pltpu.VMEM((nx, HALF, cols_out), BF16),
        pltpu.VMEM((nx, HALF, cols_out), BF16),
        *[pltpu.SemaphoreType.DMA((3, 2, max(nz, ny) - 1))] * 2,
        *[pltpu.SemaphoreType.DMA((3, 2, 2, steps))] * 2,
        *ring,
        *[pltpu.SemaphoreType.DMA((nx,))] * 2,
        *[pltpu.SemaphoreType.DMA((nx - 1,))] * 2,
        *[pltpu.SemaphoreType.DMA((max(ny - 1, 1),))] * 2,
        *[pltpu.SemaphoreType.DMA((max(nz - 1, 1),))] * 2,
        *[pltpu.SemaphoreType.DMA((max(ny - 1, 1),))] * 2,
        *[pltpu.SemaphoreType.DMA] * 2,
        *ring,
        *ring,
        *[pltpu.SemaphoreType.DMA((nx,))] * 2,
        *[pltpu.SemaphoreType.DMA((nx - 1,))] * 2,
    ]
    return pl.pallas_call(
        functools.partial(kernel, sizes),
        out_shape=jax.ShapeDtypeStruct(tok.shape, BF16),
        in_specs=[pl.BlockSpec(memory_space=pltpu.VMEM)] * 13,
        out_specs=pl.BlockSpec(memory_space=pltpu.VMEM),
        scratch_shapes=scratch,
        compiler_params=pltpu.CompilerParams(
            collective_id=0, has_side_effects=True, vmem_limit_bytes=56 * 1024 * 1024
        ),
        name="layer",
    )(
        tok,
        gin.reshape(1, width),
        wp,
        wq,
        wf,
        wv,
        maps,
        scale.reshape(1, kdim),
        lb.reshape(nx, HEAD),
        spike,
        hg.reshape(nx, HEAD),
        wpo,
        wro,
    )


def layout(devices, sizes):
    nz, ny, nx = sizes
    torus = Mesh(devices.reshape(nz, ny, nx, 2), ("z", "y", "x", "c"))
    sp = ("z", "y")
    return jax.shard_map(
        functools.partial(body, sizes),
        mesh=torus,
        in_specs=(
            P("x", ("z", "y", "c"), None),
            P(),
            P(sp, "c"),
            P(sp, "c"),
            P(sp, "c"),
            P(sp, "c"),
            P("c", None, None),
            P("c"),
            P("c"),
            P("x", sp, "c"),
            P("c"),
            P("c", sp),
            P("c", sp),
        ),
        out_specs=P("x", ("z", "y", "c"), None),
        check_vma=False,
    )


def solution(mesh):
    return layout(mesh.devices, (8, 8, mesh.shape["fs"]))
```

time: 279 us -> 84.3 us (0.30)
  waiting for transfers between devices: 159 us -> 0 us
  Pallas kernels: 0 us -> 79.3 us
  blocking collectives: 69.3 us -> 0 us
  between operations: 13.5 us -> 0.01 us
  other arithmetic: 11.6 us -> 0 us
  matrix products: 11.1 us -> 0 us
  local copies, waits for them, and re-layouts: 10 us -> 4.65 us
  starting transfers between devices: 2.81 us -> 0 us
    all_gather x4 -> x0, waiting for transfers between devices: 159 us -> none  [the longest x1 67.8 us: body(): lax.all_gather(stacked, SP, axis=0, tiled=True)]
    pallas_call x0 -> x1, Pallas kernels: none -> 79.3 us  [body(): pl.pallas_call(functools.partial(kernel, sizes), out_shape=jax.ShapeDtype...]
    all_gather x4 -> x0, blocking collectives: 60.2 us -> none  [the longest x1 27.3 us: all_blocks(): tiles = lax.all_gather(tiles, axes[k])]
    dot_general x7 -> x0, matrix products: 11.1 us -> none  [the longest x1 4.7 us: body(): jnp.dot(normed, lax.all_gather(stacked, SP, axis=0, tiled=True), preferre...]
    all_to_all x1 -> x0, blocking collectives: 9.09 us -> none  [summed_on_arrival(): lax.all_to_all(tiles, axis, split_axis=0, concat_axis=0, tiled=True)]
    transpose x2 -> x0, local copies, waits for them, and re-layouts: 6.59 us -> none  [the longest x1 6.47 us: all_blocks(): tiles = tiles.transpose(*back, *range(len(axes), tiles.ndim))]
    convert_element_type x18 -> x0, other arithmetic: 3.53 us -> none  [the longest x3 3.11 us: carried_in(): part.astype(kind)]
    unnamed x9 -> x10, local copies, waits for them, and re-layouts: 1.15 us -> 4.65 us
  transfers between devices with their start and end apart: 5 -> 0, of which waited for: 4 -> 0; matrix products, arithmetic and copies ran while one was open for 7% -> 0% of each run, Pallas kernels for 0% -> 0%
where the time goes in v1:
time: 84.3 us; the launch traced here: 83.9 us
  Pallas kernels  79.3 us (94%)
  local copies, waits for them, and re-layouts  4.65 us (6%)
    pallas_call x1, Pallas kernels, body(): pl.pallas_call(functools.partial(kernel, sizes), out_shape=jax.ShapeDtype...  79.3 us
    unnamed x10, local copies, waits for them, and re-layouts  4.65 us

profile of v1, /device:TPU:1, one launch (start us, length us, event | category | flops | bytes accessed | tf_op | source)
XLA Modules:
  0.0 83.9 jit_solution(8690124973063996232)
XLA Ops:
  0.0 0.0 copy-start.2
  0.0 0.7 copy-done.2
  0.7 0.0 copy-start
  0.7 0.7 copy.14.spike_ref
  1.4 0.0 copy-done
  1.4 0.0 copy-start.1
  1.4 0.8 copy.15.wpo_ref
  2.2 0.0 copy-done.1
  2.2 0.8 copy.16.wro_ref
  3.0 79.3 %layer.1 = bf16[1,64,2048]{2,1,0:T(8,128)(2,1)} custom-call(bf16[1,64,2048]{2,1,0:T(8,128)(2,1)} %tok_ref.1, f32[1,2048]{1,0:T(1,128)} %bitcast.4, bf16[32,512]{1,0:T(8,128)(2,1)} %wp_ref.1, bf16[32,512]{1,0:T(8,128)(2,1)} %wq_ref.1, bf16[32,512]{1,0:T(8,128)(2,1)} %wf_ref.1, bf16[32,512]{1,0:T(8,128)(2,1)} %wv_ref.1, bf16[2,256,256]{2,1,0:T(8,128)(2,1)} %maps_ref.1, ...), custom_call_target="tpu_custom_call" | custom-call | tf_op jit(solution)/shard_map/layer/pallas_call | solution.py:720
  82.3 1.7 %copy.18 = bf16[1,64,2048]{2,1,0:T(8,128)(2,1)} copy(bf16[1,64,2048]{2,1,0:T(8,128)(2,1)} %layer.1) | data formatting | bytes 524288
Async XLA Ops:
  0.0 0.7 copy-start.2
  0.7 0.8 copy-start
  1.4 0.8 copy-start.1

commit v2 on v1

--- a/solution.py
+++ b/solution.py
@@ -16,6 +16,7 @@
 WROWS = 16
 WCOLS = 256
 HALO = 16
+PARTS = 2
 EPS = 1e-06
 F32 = jnp.float32
 BF16 = jnp.bfloat16
@@ -43,20 +44,28 @@
 
 def kernel(
     sizes,
+    tok_hbm,
+    gin_hbm,
+    wp_hbm,
+    wq_hbm,
+    wf_hbm,
+    wv_hbm,
+    maps_hbm,
+    scale_hbm,
+    lb_hbm,
+    spike_hbm,
+    hg_hbm,
+    wpo_hbm,
+    wro_hbm,
+    out_ref,
     tok_ref,
     gin_ref,
-    wp_ref,
-    wq_ref,
-    wf_ref,
-    wv_ref,
     maps_ref,
     scale_ref,
     lb_ref,
     spike_ref,
     hg_ref,
-    wpo_ref,
-    wro_ref,
-    out_ref,
+    wo_ref,
     tokbuf,
     wbuf,
     wobuf,
@@ -112,11 +121,12 @@
     part_rs,
     o_ss,
     o_rs,
+    in_sems,
 ):
     nz, ny, nx = sizes
     z, y, x, c = (lax.axis_index(name) for name in ("z", "y", "x", "c"))
     sp = z * ny + y
-    width = tok_ref.shape[2]
+    width = tok_hbm.shape[2]
     wo_cols = 32 // nx
     piece = HEAD // ny
     packed = nx * piece
@@ -127,8 +137,41 @@
             src_ref=src, dst_ref=dst, send_sem=ss, recv_sem=rs, device_id=device, device_id_type=MESH
         )
 
+    def far_first(count):
+        return sorted(range(1, count), key=lambda k: -min(k, count - k))
+
     def at(base, step, count):
         return lax.rem(base + step + count, count)
+
+    pltpu.make_async_copy(tok_hbm, tok_ref, in_sems.at[0]).start()
+    lanes = pl.ds(pl.multiple_of(x * HEAD, HEAD), HEAD)
+    slices = []
+    for n, ref in enumerate((wf_hbm, wv_hbm, wp_hbm, wq_hbm)):
+        for p in range(2):
+            slices.append(
+                pltpu.make_async_copy(
+                    ref.at[p * WROWS : (p + 1) * WROWS, lanes],
+                    wbuf.at[n // 2, z, y, p, :, pl.ds((n % 2) * HEAD, HEAD)],
+                    in_sems.at[1 + 2 * n + p],
+                )
+            )
+    small = [
+        pltpu.make_async_copy(src, dst, in_sems.at[9 + n])
+        for n, (src, dst) in enumerate(
+            (
+                (gin_hbm, gin_ref),
+                (spike_hbm, spike_ref),
+                (wpo_hbm, wo_ref.at[0]),
+                (wro_hbm, wo_ref.at[1]),
+                (lb_hbm, lb_ref),
+                (hg_hbm, hg_ref),
+                (scale_hbm, scale_ref),
+                (maps_hbm, maps_ref),
+            )
+        )
+    ]
+    for copy in slices[:4] + small[:2] + slices[4:] + small[2:]:
+        copy.start()
 
     barrier = pltpu.get_barrier_semaphore()
 
@@ -154,28 +197,15 @@
         def _():
             greet(z=z - 1, y=ny - 1)
 
+    pltpu.make_async_copy(tok_hbm, tok_ref, in_sems.at[0]).wait()
+    small[0].wait()
     own = tok_ref[0].astype(F32)
     square = jnp.mean(own * own, axis=-1, keepdims=True)
     tokbuf[x, c] = (own * lax.rsqrt(square + EPS) * gin_ref[...]).astype(BF16)
-    lanes = pl.ds(pl.multiple_of(x * HEAD, HEAD), HEAD)
-    for p in range(2):
-        rows = slice(p * WROWS, (p + 1) * WROWS)
-        wbuf[0, z, y, p, :, 0:HEAD] = wf_ref[rows, lanes]
-        wbuf[0, z, y, p, :, HEAD:WCOLS] = wv_ref[rows, lanes]
-        wbuf[1, z, y, p, :, 0:HEAD] = wp_ref[rows, lanes]
-        wbuf[1, z, y, p, :, HEAD:WCOLS] = wq_ref[rows, lanes]
-    heads = spike_ref.shape[2]
-    pick = (
-        lax.broadcasted_iota(jnp.int32, (8, heads), 0)
-        == lax.broadcasted_iota(jnp.int32, (8, heads), 1)
-    ).astype(F32)
-    spbuf[x] = lax.dot_general(
-        pick,
-        spike_ref[0],
-        (((1,), (1,)), ((), ())),
-        precision=lax.Precision.HIGHEST,
-        preferred_element_type=F32,
-    )
+    small[1].wait()
+    spbuf[x] = spike_ref[0]
+    for copy in slices:
+        copy.wait()
 
     greeted = (ny - 1) + (nz - 1) + (nx - 1) + 1
     if nz > 1 and ny > 1:
@@ -202,7 +232,7 @@
         )
 
     def p1_send(st):
-        for k in range(1, max(nz, ny)):
+        for k in far_first(max(nz, ny)):
             if k < nz:
                 p1(st, k, 0)(z, at(z, k, nz)).start()
             if k < ny:
@@ -220,46 +250,55 @@
         for k in range(1, ny):
             p1(st, k, 1)(y, at(y, k, ny)).wait_send()
 
-    routes = []
-    for path, count in ((0, ny), (1, nz)):
-        for way in range(2):
-            routes.append((path, way, count // 2 if way == 0 else (count - 1) // 2))
-
-    def p2(st, path, way, step, distance, to):
+    paths = ((0, ny, nz), (1, nz, ny))
+
+    def p2(st, path, way, source, distance, part):
         sign = 1 if way == 0 else -1
         if path == 0:
-            block = wbuf.at[st, :, at(y, -sign * distance, ny), 0]
-            device = {"y": at(y, sign * to, ny)}
+            size = nz // PARTS
+            block = wbuf.at[st, pl.ds(part * size, size), at(y, -sign * source, ny), 0]
+            device = {"y": at(y, sign * max(distance - source, 1), ny)}
         else:
-            block = wbuf.at[st, at(z, -sign * distance, nz), :, 1]
-            device = {"z": at(z, sign * to, nz)}
-        return rc(
-            block, block, p2_ss.at[st, path, way, step], p2_rs.at[st, path, way, step], **device
-        )
-
-    steps = max(r[2] for r in routes)
-
-    def p2_send(st, step):
-        for path, way, count in routes:
-            if step < count:
-                p2(st, path, way, step, step, 1).start()
-
-    def p2_wait(st, step):
-        for path, way, count in routes:
-            if step < count:
-                p2(st, path, way, step, step + 1, 1).wait_recv()
-
-    def p2_advance(st, step):
-        for path, way, count in routes:
-            if step - 1 < count:
-                p2(st, path, way, step - 1, step, 1).wait_recv()
-            if step < count:
-                p2(st, path, way, step, step, 1).start()
+            size = ny // PARTS
+            block = wbuf.at[st, at(z, -sign * source, nz), pl.ds(part * size, size), 1]
+            device = {"z": at(z, sign * max(distance - source, 1), nz)}
+        where = (st, path, way, distance - 1, part)
+        return rc(block, block, p2_ss.at[where], p2_rs.at[where], **device)
+
+    def far_way(part):
+        return 0 if part < PARTS // 2 else 1
+
+    def each(part):
+        return [(path, way, part) for path in range(2) for way in range(2)]
+
+    def p2_own(st):
+        for part in range(PARTS):
+            for distance in (2, 1):
+                for path, way, _ in each(part):
+                    p2(st, path, way, 0, distance, part).start()
+
+    def p2_relay(st):
+        for part in range(PARTS):
+            for path, way, _ in each(part):
+                p2(st, path, way, 2, 2, part).wait_recv()
+                if way == far_way(part):
+                    p2(st, path, way, 2, 4, part).start()
+                p2(st, path, way, 2, 3, part).start()
+
+    def p2_wait(st):
+        for part in range(PARTS):
+            for path, way, _ in each(part):
+                p2(st, path, way, 1, 1, part).wait_recv()
+                p2(st, path, way, 3, 3, part).wait_recv()
+                if way == far_way(part):
+                    p2(st, path, way, 4, 4, part).wait_recv()
 
     def p2_done(st):
-        for path, way, count in routes:
-            for step in range(count):
-                p2(st, path, way, step, step, 1).wait_send()
+        for part in range(PARTS):
+            for path, way, _ in each(part):
+                for distance in (1, 2, 3, 4):
+                    if distance < 4 or way == far_way(part):
+                        p2(st, path, way, 0, distance, part).wait_send()
 
     right, left, across = at(x, 1, nx), at(x, -1, nx), at(x, 2, nx)
 
@@ -326,33 +365,31 @@
         spikes(k, x).start()
     p1_send(1)
 
-    wobuf[0] = wpo_ref[...].astype(F32).T
-    wobuf[1] = wro_ref[...].astype(F32).T
+    for copy in small[2:]:
+        copy.wait()
+    wobuf[...] = wo_ref[...].astype(F32)
     mine = pl.ds(pl.multiple_of(x * wo_cols, wo_cols), wo_cols)
     block = jnp.concatenate([wobuf[0, mine, :], wobuf[1, mine, :]], axis=0).astype(BF16)
     for p in range(2):
         wbuf[2, z, y, p] = block[:, p * WCOLS : (p + 1) * WCOLS]
 
     p1_wait(0)
-    p2_send(0, 0)
+    p2_own(0)
     tokens.forward()
-    p1_wait(1)
-    p2_send(1, 0)
     tokens.near()
     to_partner(1, left, c).start()
     to_partner(2, right, c).start()
+    p2_relay(0)
+    p1_wait(1)
+    p2_own(1)
     p1_send(2)
-    for step in range(1, steps):
-        p2_advance(0, step)
-        p2_advance(1, step)
-        if step == 1:
-            tokens.far()
-            to_partner(3, across, c).start()
+    tokens.far()
+    to_partner(3, across, c).start()
     for slot, owner in enumerate((x, left, right, across)):
         to_partner(slot, owner, 1 - c).wait_recv()
     for k in range(1, nx):
         spikes(k, at(x, -k, nx)).wait_recv()
-    p2_wait(0, steps - 1)
+    p2_wait(0)
 
     rows = nx * TOK
 
@@ -411,37 +448,10 @@
         to = at(y, k, ny)
         return rc(c1_send.at[to], c1_recv.at[slot], c1_ss.at[k - 1], c1_rs.at[k - 1], y=to)
 
-    for k in range(1, ny):
+    for k in far_first(ny):
         c1(k, y).start()
 
-    p1_wait(2)
-    p2_wait(1, steps - 1)
-    p2_send(2, 0)
-    projected = project(1)
-    pbuf[...] = projected[:, :HEAD].reshape(nx, TOK, HEAD)
-    qbuf[...] = projected[:, HEAD:]
-
-    last = nz * ny - 1
-    halo_src = pbuf.at[:, TOK - HALO : TOK]
-
-    def halo_copy(**device):
-        return rc(halo_src, halo, halo_ss, halo_rs, **device)
-
-    if ny > 1:
-
-        @pl.when(y < ny - 1)
-        def _():
-            halo_copy(y=y + 1).start()
-
-    if nz > 1:
-
-        @pl.when(jnp.logical_and(y == ny - 1, z < nz - 1))
-        def _():
-            halo_copy(z=z + 1, y=0).start()
-
-    @pl.when(sp == 0)
-    def _():
-        halo[...] = jnp.zeros_like(halo)
+    p2_relay(1)
 
     for k in range(1, ny):
         c1(k, at(y, -k, ny)).wait_recv()
@@ -473,6 +483,35 @@
             return _
 
         lax.fori_loop(1, nz - z, send_later, 0)
+
+    p1_wait(2)
+    p2_own(2)
+    p2_wait(1)
+    projected = project(1)
+    pbuf[...] = projected[:, :HEAD].reshape(nx, TOK, HEAD)
+    qbuf[...] = projected[:, HEAD:]
+
+    last = nz * ny - 1
+    halo_src = pbuf.at[:, TOK - HALO : TOK]
+
+    def halo_copy(**device):
+        return rc(halo_src, halo, halo_ss, halo_rs, **device)
+
+    if ny > 1:
+
+        @pl.when(y < ny - 1)
+        def _():
+            halo_copy(y=y + 1).start()
+
+    if nz > 1:
+
+        @pl.when(jnp.logical_and(y == ny - 1, z < nz - 1))
+        def _():
+            halo_copy(z=z + 1, y=0).start()
+
+    @pl.when(sp == 0)
+    def _():
+        halo[...] = jnp.zeros_like(halo)
 
     for s in range(nx):
         span = slice(s * TOK, (s + 1) * TOK)
@@ -491,9 +530,6 @@
         chosen = jnp.where(causal, scores[:, :TOK], jnp.where(before, cross, 0.0))
         within[span, :] = nn(chosen.astype(BF16), vbuf[span, :])
         cfull[span, :] = reader * jnp.exp(cfull[span, :])
-    if steps > 1:
-        p2_advance(2, 1)
-
     if ny > 1:
 
         @pl.when(y > 0)
@@ -553,19 +589,11 @@
         to = at(y, k, ny)
         return rc(c3_send.at[to], c3_recv.at[slot], c3_ss.at[k - 1], c3_rs.at[k - 1], y=to)
 
-    for k in range(1, ny):
+    for k in far_first(ny):
         c3(k, y).start()
 
     pool_ring.forward()
-    for step in range(2, steps):
-        p2_advance(2, step)
-    p2_wait(2, steps - 1)
-    for p in range(2):
-        both = wbuf[2, :, :, p].reshape(nz * ny, 2 * wo_cols, WCOLS).astype(F32)
-        cols = slice(p * WCOLS, (p + 1) * WCOLS)
-        wop[:, cols] = both[:, :wo_cols].reshape(nz * ny * wo_cols, WCOLS).astype(BF16)
-        wor[:, cols] = both[:, wo_cols:].reshape(nz * ny * wo_cols, WCOLS).astype(BF16)
-
+    p2_relay(2)
     for k in range(1, ny):
         c3(k, at(y, -k, ny)).wait_recv()
     gain = hg_ref[pl.ds(x, 1), :]
@@ -580,7 +608,6 @@
     for s in range(nx):
         finish(s)
     rec_ring.start()
-
     pool_ring.near()
     pool_ring.far()
     pieces = []
@@ -589,31 +616,38 @@
         diff = jnp.concatenate([xpool[2 * g], xpool[2 * g + 1]], axis=1)
         pieces.append((nn(diff, maps_ref[g]) * scale_ref[:, cols]).astype(BF16))
     rec_ring.forward()
+    p2_wait(2)
+    for p in range(2):
+        both = wbuf[2, :, :, p].reshape(nz * ny, 2 * wo_cols, WCOLS).astype(F32)
+        cols = slice(p * WCOLS, (p + 1) * WCOLS)
+        wop[:, cols] = both[:, :wo_cols].reshape(nz * ny * wo_cols, WCOLS).astype(BF16)
+        wor[:, cols] = both[:, wo_cols:].reshape(nz * ny * wo_cols, WCOLS).astype(BF16)
     pacc[...] = nt(jnp.concatenate(pieces, axis=1), wop[...])
     rec_ring.near()
     rec_ring.far()
-    rec = jnp.concatenate([xrec[i] for i in range(nx)], axis=1)
     cols_out = nz * ny * wo_cols
-    parts[...] = (
-        (pacc[...] + nt(rec, wor[...])).astype(BF16).reshape(nx, 2, HALF, cols_out)
-    )
 
     def to_half(s):
         return rc(parts.at[s, 1 - c], part_in.at[s], part_ss.at[s], part_rs.at[s], c=1 - c)
-
-    for s in range(nx):
-        to_half(s).start()
 
     def deliver(k, owner):
         to = at(x, k, nx)
         return rc(mixed.at[to], obuf.at[owner], o_ss.at[k - 1], o_rs.at[k - 1], x=to)
 
-    for s in range(nx):
+    order_x = (*far_first(nx), 0)
+    rec = jnp.concatenate([xrec[i] for i in range(nx)], axis=1)
+    parts[...] = (pacc[...] + nt(rec, wor[...])).astype(BF16).reshape(nx, 2, HALF, cols_out)
+    for k in order_x:
+        to_half(at(x, k, nx)).start()
+    for k in order_x:
+        s = at(x, k, nx)
         to_half(s).wait_recv()
-        mixed[s] = (parts[s, c].astype(F32) + part_in[s].astype(F32)).astype(BF16)
-    for k in range(1, nx):
-        deliver(k, x).start()
-    obuf[x] = mixed[x]
+        joint = (parts[s, c].astype(F32) + part_in[s].astype(F32)).astype(BF16)
+        if k:
+            mixed[s] = joint
+            deliver(k, x).start()
+        else:
+            obuf[x] = joint
     for k in range(1, nx):
         deliver(k, at(x, -k, nx)).wait_recv()
 
@@ -671,15 +705,25 @@
     wo_cols = 32 // nx
     cols_out = nz * ny * wo_cols
     kdim = nx * HEAD
-    steps = max(ny // 2, nz // 2)
     ring = [pltpu.SemaphoreType.DMA((6,))] * 2
+    ring_inputs = [
+        pltpu.VMEM(tok.shape, BF16),
+        pltpu.VMEM((1, width), F32),
+        pltpu.VMEM(maps.shape, BF16),
+        pltpu.VMEM((1, kdim), F32),
+        pltpu.VMEM((nx, HEAD), F32),
+        pltpu.VMEM((1, spike.shape[2], TOK), F32),
+        pltpu.VMEM((nx, HEAD), F32),
+        pltpu.VMEM((2, 32, kdim), BF16),
+    ]
     scratch = [
+        *ring_inputs,
         pltpu.VMEM((nx, 2, HALF, width), BF16),
         pltpu.VMEM((3, nz, ny, 2, WROWS, WCOLS), BF16),
         pltpu.VMEM((2, 32, kdim), F32),
         pltpu.VMEM((cols_out, kdim), BF16),
         pltpu.VMEM((cols_out, kdim), BF16),
-        pltpu.VMEM((nx, 8, TOK), F32),
+        pltpu.VMEM((nx, spike.shape[2], TOK), F32),
         pltpu.VMEM((rows, HEAD), BF16),
         pltpu.VMEM((rows, HEAD), BF16),
         pltpu.VMEM((rows, HEAD), BF16),
@@ -704,7 +748,7 @@
         pltpu.VMEM((nx, HALF, cols_out), BF16),
         pltpu.VMEM((nx, HALF, cols_out), BF16),
         *[pltpu.SemaphoreType.DMA((3, 2, max(nz, ny) - 1))] * 2,
-        *[pltpu.SemaphoreType.DMA((3, 2, 2, steps))] * 2,
+        *[pltpu.SemaphoreType.DMA((3, 2, 2, 4, PARTS))] * 2,
         *ring,
         *[pltpu.SemaphoreType.DMA((nx,))] * 2,
         *[pltpu.SemaphoreType.DMA((nx - 1,))] * 2,
@@ -716,11 +760,12 @@
         *ring,
         *[pltpu.SemaphoreType.DMA((nx,))] * 2,
         *[pltpu.SemaphoreType.DMA((nx - 1,))] * 2,
+        pltpu.SemaphoreType.DMA((17,)),
     ]
     return pl.pallas_call(
         functools.partial(kernel, sizes),
         out_shape=jax.ShapeDtypeStruct(tok.shape, BF16),
-        in_specs=[pl.BlockSpec(memory_space=pltpu.VMEM)] * 13,
+        in_specs=[pl.BlockSpec(memory_space=pltpu.HBM)] * 13,
         out_specs=pl.BlockSpec(memory_space=pltpu.VMEM),
         scratch_shapes=scratch,
         compiler_params=pltpu.CompilerParams(
@@ -737,10 +782,10 @@
         maps,
         scale.reshape(1, kdim),
         lb.reshape(nx, HEAD),
-        spike,
+        jnp.swapaxes(spike, 1, 2),
         hg.reshape(nx, HEAD),
-        wpo,
-        wro,
+        wpo.T,
+        wro.T,
     )
 
 

time: 84.3 us -> 72.6 us (0.86)
  Pallas kernels: 79.3 us -> 70.8 us
  local copies, waits for them, and re-layouts: 4.65 us -> 1.67 us
    pallas_call x1, Pallas kernels: 79.3 us -> 70.8 us  [body(): pl.pallas_call(functools.partial(kernel, sizes), out_shape=jax.ShapeDtype...]
    unnamed x10 -> x1, local copies, waits for them, and re-layouts: 4.65 us -> 1.67 us
where the time goes in v2:
time: 72.6 us; the launch traced here: 72.5 us
  Pallas kernels  70.8 us (98%)
  local copies, waits for them, and re-layouts  1.67 us (2%)
    pallas_call x1, Pallas kernels, body(): pl.pallas_call(functools.partial(kernel, sizes), out_shape=jax.ShapeDtype...  70.8 us
    unnamed x1, local copies, waits for them, and re-layouts  1.67 us

profile of v2, /device:TPU:1, one launch (start us, length us, event | category | flops | bytes accessed | tf_op | source)
XLA Modules:
  0.0 72.5 jit_solution(1902376233510009588)
XLA Ops:
  0.0 70.8 %layer.1 = bf16[1,64,2048]{2,1,0:T(8,128)(2,1)} custom-call(bf16[1,64,2048]{2,1,0:T(8,128)(2,1)} %tok_hbm.1, f32[1,2048]{1,0:T(1,128)} %bitcast.9, bf16[32,512]{1,0:T(8,128)(2,1)} %wp_hbm.1, bf16[32,512]{1,0:T(8,128)(2,1)} %wq_hbm.1, bf16[32,512]{1,0:T(8,128)(2,1)} %wf_hbm.1, bf16[32,512]{1,0:T(8,128)(2,1)} %wv_hbm.1, bf16[2,256,256]{2,1,0:T(8,128)(2,1)} %maps_hbm.1, ...), custom_call_target="tpu_custom_call" | custom-call | tf_op jit(solution)/shard_map/layer/pallas_call | solution.py:765
  70.8 1.7 %copy.15 = bf16[1,64,2048]{2,1,0:T(8,128)(2,1)} copy(bf16[1,64,2048]{2,1,0:T(8,128)(2,1)} %layer.1) | data formatting | bytes 524288

commit v3 on v2

--- a/solution.py
+++ b/solution.py
@@ -68,6 +68,7 @@
     wo_ref,
     tokbuf,
     wbuf,
+    wqp,
     wobuf,
     wop,
     wor,
@@ -98,7 +99,8 @@
     p1_ss,
     p1_rs,
     p2_ss,
-    p2_rs,
+    p2_near,
+    p2_rest,
     tok_ss,
     tok_rs,
     d2d_ss,
@@ -137,6 +139,12 @@
             src_ref=src, dst_ref=dst, send_sem=ss, recv_sem=rs, device_id=device, device_id_type=MESH
         )
 
+    def taken(sem, ref):
+        rc(ref, ref, sp_ss, sem, c=1 - c).wait_recv()
+
+    def left_here(sem, ref):
+        rc(ref, ref, sem, sp_rs, c=1 - c).wait_send()
+
     def far_first(count):
         return sorted(range(1, count), key=lambda k: -min(k, count - k))
 
@@ -146,17 +154,24 @@
     pltpu.make_async_copy(tok_hbm, tok_ref, in_sems.at[0]).start()
     lanes = pl.ds(pl.multiple_of(x * HEAD, HEAD), HEAD)
     slices = []
-    for n, ref in enumerate((wf_hbm, wv_hbm, wp_hbm, wq_hbm)):
+    for n, ref in enumerate((wf_hbm, wv_hbm)):
         for p in range(2):
             slices.append(
                 pltpu.make_async_copy(
                     ref.at[p * WROWS : (p + 1) * WROWS, lanes],
-                    wbuf.at[n // 2, z, y, p, :, pl.ds((n % 2) * HEAD, HEAD)],
-                    in_sems.at[1 + 2 * n + p],
+                    wbuf.at[0, z, y, p, :, pl.ds(n * HEAD, HEAD)],
+                    in_sems.at[1],
                 )
             )
+    for n, ref in enumerate((wq_hbm, wp_hbm)):
+        slices.append(
+            pltpu.make_async_copy(ref.at[:, lanes], wqp.at[n, z, y], in_sems.at[2])
+        )
+    def fetched(n):
+        pltpu.make_async_copy(wbuf.at[0, z, y], wbuf.at[0, z, y], in_sems.at[n]).wait()
+
     small = [
-        pltpu.make_async_copy(src, dst, in_sems.at[9 + n])
+        pltpu.make_async_copy(src, dst, in_sems.at[3 + min(n, 2) if n < 4 else n + 2])
         for n, (src, dst) in enumerate(
             (
                 (gin_hbm, gin_ref),
@@ -197,6 +212,126 @@
         def _():
             greet(z=z - 1, y=ny - 1)
 
+    greeted = (ny - 1) + (nz - 1) + (nx - 1) + 1
+    if nz > 1 and ny > 1:
+        at_end = (y // (ny - 1)) * (1 - z // (nz - 1))
+        at_start = ((ny - 1 - y) // (ny - 1)) * (1 - (nz - 1 - z) // (nz - 1))
+        greeted = greeted + at_end + at_start
+    fetched(1)
+    pl.semaphore_wait(barrier, greeted)
+
+    def wslot(st, path, zz, yy):
+        return wqp.at[path, zz, yy] if st == 1 else wbuf.at[st // 2, zz, yy, path]
+
+    def p1(st, k, path):
+        if path == 0:
+            return lambda zz, zt: rc(
+                wslot(st, 0, zz, y),
+                wslot(st, 0, zz, y),
+                p1_ss.at[st],
+                p1_rs.at[st],
+                z=zt,
+            )
+        return lambda yy, yt: rc(
+            wslot(st, 1, z, yy),
+            wslot(st, 1, z, yy),
+            p1_ss.at[st],
+            p1_rs.at[st],
+            y=yt,
+        )
+
+    def p1_send(st):
+        for k in far_first(max(nz, ny)):
+            if k < nz:
+                p1(st, k, 0)(z, at(z, k, nz)).start()
+            if k < ny:
+                p1(st, k, 1)(y, at(y, k, ny)).start()
+
+    def p1_wait(st):
+        taken(p1_rs.at[st], wbuf.at[0, 0, 0 : ny - 1])
+
+    def p1_done(st):
+        left_here(p1_ss.at[st], wbuf.at[0, 0, 0 : ny - 1])
+
+    paths = ((0, ny, nz), (1, nz, ny))
+
+    def p2(st, path, way, source, distance, part):
+        sign = 1 if way == 0 else -1
+        if path == 0:
+            size = nz // PARTS
+            block = wslot(st, 0, pl.ds(part * size, size), at(y, -sign * source, ny))
+            device = {"y": at(y, sign * max(distance - source, 1), ny)}
+        else:
+            size = ny // PARTS
+            block = wslot(st, 1, at(z, -sign * source, nz), pl.ds(part * size, size))
+            device = {"z": at(z, sign * max(distance - source, 1), nz)}
+        arrives = p2_near.at[st, part] if distance == 2 else p2_rest.at[st, path]
+        return rc(block, block, p2_ss.at[st], arrives, **device)
+
+    def far_way(part):
+        return 0 if part < PARTS // 2 else 1
+
+    def each(part):
+        return [(path, way, part) for path in range(2) for way in range(2)]
+
+    def p2_own(st):
+        for part in range(PARTS):
+            for distance in (2, 1):
+                for path, way, _ in each(part):
+                    p2(st, path, way, 0, distance, part).start()
+
+    def p2_relay(st):
+        for part in range(PARTS):
+            taken(p2_near.at[st, part], wbuf.at[0, 0, 0 : 2 * ny // PARTS])
+            for path, way, _ in each(part):
+                if way == far_way(part):
+                    p2(st, path, way, 2, 4, part).start()
+                p2(st, path, way, 2, 3, part).start()
+
+    def p2_wait(st, only=(0, 1)):
+        for path in only:
+            taken(p2_rest.at[st, path], wbuf.at[0, 0:5, 0 : ny // 2])
+
+    def p2_done(st):
+        left_here(p2_ss.at[st], wbuf.at[0, 0 : nz - 1])
+
+    right, left, across = at(x, 1, nx), at(x, -1, nx), at(x, 2, nx)
+
+    def token_half(kind, owner, half, to):
+        ref = tokbuf.at[owner, c, pl.ds(half * (HALF // 2), HALF // 2)]
+        return rc(ref, ref, tok_ss, tok_rs.at[kind], x=to)
+
+    def tokens_start():
+        token_half(0, x, 0, right).start()
+        token_half(1, x, 1, left).start()
+        token_half(2, x, 1, right).start()
+        token_half(2, x, 0, left).start()
+
+    def tokens_forward():
+        token_half(0, left, 0, right).wait_recv()
+        token_half(3, left, 0, right).start()
+        token_half(1, right, 1, left).wait_recv()
+        token_half(3, right, 1, left).start()
+
+    def tokens_near():
+        taken(tok_rs.at[2], tokbuf.at[0, 0])
+
+    def tokens_far():
+        taken(tok_rs.at[3], tokbuf.at[0, 0])
+
+    def to_all_x(ref_of, ss, rs):
+        for k in (2, 1, 3):
+            rc(ref_of(x), ref_of(x), ss, rs, x=at(x, k, nx)).start()
+
+    def to_partner(owner, core):
+        return rc(
+            tokbuf.at[owner, core], tokbuf.at[owner, core], d2d_ss, d2d_rs, c=1 - c
+        )
+
+    def spikes(k, owner):
+        return rc(spbuf.at[owner], spbuf.at[owner], sp_ss, sp_rs, x=at(x, k, nx))
+
+    p1_send(0)
     pltpu.make_async_copy(tok_hbm, tok_ref, in_sems.at[0]).wait()
     small[0].wait()
     own = tok_ref[0].astype(F32)
@@ -204,199 +339,44 @@
     tokbuf[x, c] = (own * lax.rsqrt(square + EPS) * gin_ref[...]).astype(BF16)
     small[1].wait()
     spbuf[x] = spike_ref[0]
-    for copy in slices:
-        copy.wait()
-
-    greeted = (ny - 1) + (nz - 1) + (nx - 1) + 1
-    if nz > 1 and ny > 1:
-        at_end = (y // (ny - 1)) * (1 - z // (nz - 1))
-        at_start = ((ny - 1 - y) // (ny - 1)) * (1 - (nz - 1 - z) // (nz - 1))
-        greeted = greeted + at_end + at_start
-    pl.semaphore_wait(barrier, greeted)
-
-    def p1(st, k, path):
-        if path == 0:
-            return lambda zz, zt: rc(
-                wbuf.at[st, zz, y, 0],
-                wbuf.at[st, zz, y, 0],
-                p1_ss.at[st, 0, k - 1],
-                p1_rs.at[st, 0, k - 1],
-                z=zt,
-            )
-        return lambda yy, yt: rc(
-            wbuf.at[st, z, yy, 1],
-            wbuf.at[st, z, yy, 1],
-            p1_ss.at[st, 1, k - 1],
-            p1_rs.at[st, 1, k - 1],
-            y=yt,
-        )
-
-    def p1_send(st):
-        for k in far_first(max(nz, ny)):
-            if k < nz:
-                p1(st, k, 0)(z, at(z, k, nz)).start()
-            if k < ny:
-                p1(st, k, 1)(y, at(y, k, ny)).start()
-
-    def p1_wait(st):
-        for k in range(1, nz):
-            p1(st, k, 0)(at(z, -k, nz), at(z, -k, nz)).wait_recv()
-        for k in range(1, ny):
-            p1(st, k, 1)(at(y, -k, ny), at(y, -k, ny)).wait_recv()
-
-    def p1_done(st):
-        for k in range(1, nz):
-            p1(st, k, 0)(z, at(z, k, nz)).wait_send()
-        for k in range(1, ny):
-            p1(st, k, 1)(y, at(y, k, ny)).wait_send()
-
-    paths = ((0, ny, nz), (1, nz, ny))
-
-    def p2(st, path, way, source, distance, part):
-        sign = 1 if way == 0 else -1
-        if path == 0:
-            size = nz // PARTS
-            block = wbuf.at[st, pl.ds(part * size, size), at(y, -sign * source, ny), 0]
-            device = {"y": at(y, sign * max(distance - source, 1), ny)}
-        else:
-            size = ny // PARTS
-            block = wbuf.at[st, at(z, -sign * source, nz), pl.ds(part * size, size), 1]
-            device = {"z": at(z, sign * max(distance - source, 1), nz)}
-        where = (st, path, way, distance - 1, part)
-        return rc(block, block, p2_ss.at[where], p2_rs.at[where], **device)
-
-    def far_way(part):
-        return 0 if part < PARTS // 2 else 1
-
-    def each(part):
-        return [(path, way, part) for path in range(2) for way in range(2)]
-
-    def p2_own(st):
-        for part in range(PARTS):
-            for distance in (2, 1):
-                for path, way, _ in each(part):
-                    p2(st, path, way, 0, distance, part).start()
-
-    def p2_relay(st):
-        for part in range(PARTS):
-            for path, way, _ in each(part):
-                p2(st, path, way, 2, 2, part).wait_recv()
-                if way == far_way(part):
-                    p2(st, path, way, 2, 4, part).start()
-                p2(st, path, way, 2, 3, part).start()
-
-    def p2_wait(st):
-        for part in range(PARTS):
-            for path, way, _ in each(part):
-                p2(st, path, way, 1, 1, part).wait_recv()
-                p2(st, path, way, 3, 3, part).wait_recv()
-                if way == far_way(part):
-                    p2(st, path, way, 4, 4, part).wait_recv()
-
-    def p2_done(st):
-        for part in range(PARTS):
-            for path, way, _ in each(part):
-                for distance in (1, 2, 3, 4):
-                    if distance < 4 or way == far_way(part):
-                        p2(st, path, way, 0, distance, part).wait_send()
-
-    right, left, across = at(x, 1, nx), at(x, -1, nx), at(x, 2, nx)
-
-    def ring_x(part, ss, rs):
-        def move(slot, owner, half, to):
-            return rc(part(owner, half), part(owner, half), ss.at[slot], rs.at[slot], x=to)
-
-        class Ring:
-            def start_first(self):
-                move(0, x, 0, right).start()
-                move(2, x, 1, left).start()
-
-            def start_second(self):
-                move(1, x, 1, right).start()
-                move(3, x, 0, left).start()
-
-            def start(self):
-                self.start_first()
-                self.start_second()
-
-            def forward(self):
-                move(0, left, 0, right).wait_recv()
-                move(4, left, 0, right).start()
-                move(2, right, 1, left).wait_recv()
-                move(5, right, 1, left).start()
-
-            def near(self):
-                move(1, left, 1, right).wait_recv()
-                move(3, right, 0, left).wait_recv()
-
-            def far(self):
-                move(4, across, 0, right).wait_recv()
-                move(5, across, 1, left).wait_recv()
-
-            def done(self):
-                for slot, owner, half, to in (
-                    (0, x, 0, right),
-                    (1, x, 1, right),
-                    (2, x, 1, left),
-                    (3, x, 0, left),
-                    (4, left, 0, right),
-                    (5, right, 1, left),
-                ):
-                    move(slot, owner, half, to).wait_send()
-
-        return Ring()
-
-    tokens = ring_x(
-        lambda owner, half: tokbuf.at[owner, c, pl.ds(half * (HALF // 2), HALF // 2)], tok_ss, tok_rs
-    )
-
-    def to_partner(slot, owner, core):
-        return rc(
-            tokbuf.at[owner, core], tokbuf.at[owner, core], d2d_ss.at[slot], d2d_rs.at[slot], c=1 - c
-        )
-
-    def spikes(k, owner):
-        return rc(spbuf.at[owner], spbuf.at[owner], sp_ss.at[k - 1], sp_rs.at[k - 1], x=at(x, k, nx))
-
-    p1_send(0)
-    tokens.start()
-    to_partner(0, x, c).start()
+    fetched(2)
+    tokens_start()
+    to_partner(x, c).start()
     for k in range(1, nx):
         spikes(k, x).start()
     p1_send(1)
 
-    for copy in small[2:]:
+    pltpu.make_async_copy(wo_ref, wo_ref, in_sems.at[5]).wait()
+    for copy in small[4:]:
         copy.wait()
     wobuf[...] = wo_ref[...].astype(F32)
     mine = pl.ds(pl.multiple_of(x * wo_cols, wo_cols), wo_cols)
     block = jnp.concatenate([wobuf[0, mine, :], wobuf[1, mine, :]], axis=0).astype(BF16)
     for p in range(2):
-        wbuf[2, z, y, p] = block[:, p * WCOLS : (p + 1) * WCOLS]
+        wbuf[1, z, y, p] = block[:, p * WCOLS : (p + 1) * WCOLS]
 
     p1_wait(0)
     p2_own(0)
-    tokens.forward()
-    tokens.near()
-    to_partner(1, left, c).start()
-    to_partner(2, right, c).start()
+    tokens_forward()
+    tokens_near()
+    to_partner(left, c).start()
+    to_partner(right, c).start()
     p2_relay(0)
     p1_wait(1)
     p2_own(1)
     p1_send(2)
-    tokens.far()
-    to_partner(3, across, c).start()
-    for slot, owner in enumerate((x, left, right, across)):
-        to_partner(slot, owner, 1 - c).wait_recv()
-    for k in range(1, nx):
-        spikes(k, at(x, -k, nx)).wait_recv()
+    tokens_far()
+    to_partner(across, c).start()
+    taken(d2d_rs, tokbuf.at[:, 0])
+    taken(sp_rs, spbuf.at[0 : nx - 1])
     p2_wait(0)
 
     rows = nx * TOK
 
-    def project(st):
-        return nn(tokbuf[...].reshape(rows, width), wbuf[st].reshape(width, WCOLS)).astype(BF16)
-
-    projected = project(0)
+    def project(weights):
+        return nn(tokbuf[...].reshape(rows, width), weights).astype(BF16)
+
+    projected = project(wbuf[0].reshape(width, WCOLS))
     fbuf[...] = projected[:, :HEAD]
     vbuf[...] = projected[:, HEAD:]
 
@@ -409,27 +389,33 @@
     ones_b = jnp.ones((TOK, HEAD), BF16)
     second = lax.broadcasted_iota(jnp.int32, (TOK, HEAD), 0) >= BLOCK
     lb_gate = 1.0 / (1.0 + jnp.exp(lb_ref[pl.ds(x, 1), :]))
-    decays = []
+    keys = lb_gate * (1.0 / (1.0 + jnp.exp(fbuf[...].astype(F32))))
+    logs = three_parts(jnp.log(1.0 - keys))
+    inners = []
     for s in range(nx):
         span = slice(s * TOK, (s + 1) * TOK)
-        key = lb_gate * (1.0 / (1.0 + jnp.exp(fbuf[span, :].astype(F32))))
-        logs = three_parts(jnp.log1p(-key))
-        spike_row = spbuf[s, pl.ds(x, 1), :]
-        spread = three_parts(lower * spike_row)
-        inner = nn(
-            jnp.concatenate([lower_b, lower_b, lower_b, *spread], axis=1),
-            jnp.concatenate([*logs, ones_b, ones_b, ones_b], axis=0),
+        spread = three_parts(lower * spbuf[s, pl.ds(x, 1), :])
+        inners.append(
+            nn(
+                jnp.concatenate([lower_b, lower_b, lower_b, *spread], axis=1),
+                jnp.concatenate([*(part[span] for part in logs), ones_b, ones_b, ones_b], axis=0),
+            )
         )
+    decays, tails = [], []
+    for s in range(nx):
+        span = slice(s * TOK, (s + 1) * TOK)
+        inner = inners[s]
         first_end = inner[BLOCK - 1 : BLOCK, :]
         total = first_end + inner[TOK - 1 : TOK, :]
         full = inner + jnp.where(second, first_end, 0.0)
         inner_buf[span, :] = inner
         cfull[span, :] = full
-        tail = (key * jnp.exp(total - full)).astype(BF16)
-        state = tn(vbuf[span, :], tail).astype(BF16)
+        tails.append((keys[span] * jnp.exp(total - full)).astype(BF16))
+        decays.append(jnp.exp(total))
+    for s in range(nx):
+        state = tn(vbuf[s * TOK : (s + 1) * TOK, :], tails[s]).astype(BF16)
         for j in range(ny):
             c1_send[j, s * piece : (s + 1) * piece, :] = state[j * piece : (j + 1) * piece, :]
-        decays.append(jnp.exp(total))
 
     def decay_rows(values):
         out = []
@@ -446,15 +432,14 @@
 
     def c1(k, slot):
         to = at(y, k, ny)
-        return rc(c1_send.at[to], c1_recv.at[slot], c1_ss.at[k - 1], c1_rs.at[k - 1], y=to)
+        return rc(c1_send.at[to], c1_recv.at[slot], c1_ss, c1_rs, y=to)
 
     for k in far_first(ny):
         c1(k, y).start()
 
     p2_relay(1)
 
-    for k in range(1, ny):
-        c1(k, at(y, -k, ny)).wait_recv()
+    taken(c1_rs, c1_send.at[0 : ny - 1])
 
     def read_decay(block, s):
         at_row = packed + 2 * s
@@ -486,10 +471,8 @@
 
     p1_wait(2)
     p2_own(2)
-    p2_wait(1)
-    projected = project(1)
-    pbuf[...] = projected[:, :HEAD].reshape(nx, TOK, HEAD)
-    qbuf[...] = projected[:, HEAD:]
+    p2_wait(1, (1,))
+    pbuf[...] = project(wqp[1].reshape(width, HEAD)).reshape(nx, TOK, HEAD)
 
     last = nz * ny - 1
     halo_src = pbuf.at[:, TOK - HALO : TOK]
@@ -512,6 +495,9 @@
     @pl.when(sp == 0)
     def _():
         halo[...] = jnp.zeros_like(halo)
+
+    p2_wait(1, (0,))
+    qbuf[...] = project(wqp[0].reshape(width, HEAD))
 
     for s in range(nx):
         span = slice(s * TOK, (s + 1) * TOK)
@@ -554,14 +540,7 @@
         sums = nn(band, pbuf[s]) + nn(band_before, halo[s])
         xpool[x, s * TOK : (s + 1) * TOK, :] = (sums / count - pbuf[s].astype(F32)).astype(BF16)
 
-    half_rows = rows // 2
-    pool_ring = ring_x(
-        lambda owner, half: xpool.at[owner, pl.ds(half * half_rows, half_rows)], xp_ss, xp_rs
-    )
-    rec_ring = ring_x(
-        lambda owner, half: xrec.at[owner, pl.ds(half * half_rows, half_rows)], xr_ss, xr_rs
-    )
-    pool_ring.start()
+    to_all_x(lambda owner: xpool.at[owner], xp_ss, xp_rs)
 
     def add_row(zz, carry):
         if nz > 1:
@@ -587,15 +566,13 @@
 
     def c3(k, slot):
         to = at(y, k, ny)
-        return rc(c3_send.at[to], c3_recv.at[slot], c3_ss.at[k - 1], c3_rs.at[k - 1], y=to)
+        return rc(c3_send.at[to], c3_recv.at[slot], c3_ss, c3_rs, y=to)
 
     for k in far_first(ny):
         c3(k, y).start()
 
-    pool_ring.forward()
     p2_relay(2)
-    for k in range(1, ny):
-        c3(k, at(y, -k, ny)).wait_recv()
+    taken(c3_rs, c3_send.at[0 : ny - 1])
     gain = hg_ref[pl.ds(x, 1), :]
 
     def finish(s):
@@ -603,42 +580,46 @@
         prior = c3_recv[:, s * piece : (s + 1) * piece, :].reshape(HEAD, HEAD)
         read = within[span, :] + nt(cfull[span, :].astype(BF16), prior)
         square = jnp.mean(read * read, axis=-1, keepdims=True)
-        xrec[x, span, :] = (read * lax.rsqrt(square + EPS) * gain).astype(BF16)
+        normal = (read * lax.rsqrt(square + EPS) * gain).astype(BF16)
+        xrec[x, s] = normal.reshape(2, HALF, HEAD)
 
     for s in range(nx):
         finish(s)
-    rec_ring.start()
-    pool_ring.near()
-    pool_ring.far()
+    to_all_x(lambda owner: xrec.at[owner], xr_ss, xr_rs)
+    taken(xp_rs, xpool.at[0 : nx - 1])
     pieces = []
     for g in range(half_pool // WCOLS):
         cols = slice(g * WCOLS, (g + 1) * WCOLS)
         diff = jnp.concatenate([xpool[2 * g], xpool[2 * g + 1]], axis=1)
         pieces.append((nn(diff, maps_ref[g]) * scale_ref[:, cols]).astype(BF16))
-    rec_ring.forward()
     p2_wait(2)
     for p in range(2):
-        both = wbuf[2, :, :, p].reshape(nz * ny, 2 * wo_cols, WCOLS).astype(F32)
+        both = wbuf[1, :, :, p].reshape(nz * ny, 2 * wo_cols, WCOLS).astype(F32)
         cols = slice(p * WCOLS, (p + 1) * WCOLS)
         wop[:, cols] = both[:, :wo_cols].reshape(nz * ny * wo_cols, WCOLS).astype(BF16)
         wor[:, cols] = both[:, wo_cols:].reshape(nz * ny * wo_cols, WCOLS).astype(BF16)
-    pacc[...] = nt(jnp.concatenate(pieces, axis=1), wop[...])
-    rec_ring.near()
-    rec_ring.far()
+    pooled_out = nt(jnp.concatenate(pieces, axis=1), wop[...])
+    pacc[...] = pooled_out.reshape(nx, 2, HALF, nz * ny * wo_cols)
+    taken(xr_rs, xrec.at[0 : nx - 1])
     cols_out = nz * ny * wo_cols
 
     def to_half(s):
-        return rc(parts.at[s, 1 - c], part_in.at[s], part_ss.at[s], part_rs.at[s], c=1 - c)
+        return rc(parts.at[s, 1 - c], part_in.at[s], part_ss, part_rs.at[s], c=1 - c)
 
     def deliver(k, owner):
         to = at(x, k, nx)
-        return rc(mixed.at[to], obuf.at[owner], o_ss.at[k - 1], o_rs.at[k - 1], x=to)
+        return rc(mixed.at[to], obuf.at[owner], o_ss, o_rs, x=to)
 
     order_x = (*far_first(nx), 0)
-    rec = jnp.concatenate([xrec[i] for i in range(nx)], axis=1)
-    parts[...] = (pacc[...] + nt(rec, wor[...])).astype(BF16).reshape(nx, 2, HALF, cols_out)
+    def half_of(core):
+        rec = jnp.concatenate([xrec[i, :, core].reshape(nx * HALF, HEAD) for i in range(nx)], axis=1)
+        pooled = pacc[:, core].reshape(nx * HALF, cols_out)
+        parts[:, core] = (pooled + nt(rec, wor[...])).astype(BF16).reshape(nx, HALF, cols_out)
+
+    half_of(1 - c)
     for k in order_x:
         to_half(at(x, k, nx)).start()
+    half_of(c)
     for k in order_x:
         s = at(x, k, nx)
         to_half(s).wait_recv()
@@ -648,8 +629,7 @@
             deliver(k, x).start()
         else:
             obuf[x] = joint
-    for k in range(1, nx):
-        deliver(k, at(x, -k, nx)).wait_recv()
+    taken(o_rs, mixed.at[0 : nx - 1])
 
     chunk = min(HEAD, cols_out)
     total_cols = chunk * nx
@@ -669,17 +649,15 @@
     for st in range(3):
         p1_done(st)
         p2_done(st)
-    tokens.done()
-    pool_ring.done()
-    rec_ring.done()
-    for slot, owner in enumerate((x, left, right, across)):
-        to_partner(slot, owner, c).wait_send()
-    for k in range(1, nx):
-        spikes(k, x).wait_send()
-        deliver(k, x).wait_send()
-    for k in range(1, ny):
-        c1(k, y).wait_send()
-        c3(k, y).wait_send()
+    left_here(tok_ss, tokbuf.at[0:3, 0])
+    left_here(d2d_ss, tokbuf.at[:, 0])
+    left_here(sp_ss, spbuf.at[0 : nx - 1])
+    left_here(c1_ss, c1_send.at[0 : ny - 1])
+    left_here(c3_ss, c3_send.at[0 : ny - 1])
+    left_here(xp_ss, xpool.at[0 : nx - 1])
+    left_here(xr_ss, xrec.at[0 : nx - 1])
+    left_here(o_ss, mixed.at[0 : nx - 1])
+    left_here(part_ss, part_in)
     if nz > 1:
 
         def sent_later(k, _):
@@ -687,9 +665,6 @@
             return _
 
         lax.fori_loop(1, nz - z, sent_later, 0)
-    for s in range(nx):
-        to_half(s).wait_send()
-
     @pl.when(sp < last)
     def _():
         halo_copy(c=1 - c).wait_send()
@@ -705,7 +680,6 @@
     wo_cols = 32 // nx
     cols_out = nz * ny * wo_cols
     kdim = nx * HEAD
-    ring = [pltpu.SemaphoreType.DMA((6,))] * 2
     ring_inputs = [
         pltpu.VMEM(tok.shape, BF16),
         pltpu.VMEM((1, width), F32),
@@ -719,7 +693,8 @@
     scratch = [
         *ring_inputs,
         pltpu.VMEM((nx, 2, HALF, width), BF16),
-        pltpu.VMEM((3, nz, ny, 2, WROWS, WCOLS), BF16),
+        pltpu.VMEM((2, nz, ny, 2, WROWS, WCOLS), BF16),
+        pltpu.VMEM((2, nz, ny, 2 * WROWS, HEAD), BF16),
         pltpu.VMEM((2, 32, kdim), F32),
         pltpu.VMEM((cols_out, kdim), BF16),
         pltpu.VMEM((cols_out, kdim), BF16),
@@ -741,26 +716,30 @@
         pltpu.VMEM((nx, HALO, HEAD), BF16),
         pltpu.VMEM((rows, HEAD), F32),
         pltpu.VMEM((nx, rows, HEAD), BF16),
-        pltpu.VMEM((nx, rows, HEAD), BF16),
-        pltpu.VMEM((rows, cols_out), F32),
+        pltpu.VMEM((nx, nx, 2, HALF, HEAD), BF16),
+        pltpu.VMEM((nx, 2, HALF, cols_out), F32),
         pltpu.VMEM((nx, 2, HALF, cols_out), BF16),
         pltpu.VMEM((nx, HALF, cols_out), BF16),
         pltpu.VMEM((nx, HALF, cols_out), BF16),
         pltpu.VMEM((nx, HALF, cols_out), BF16),
-        *[pltpu.SemaphoreType.DMA((3, 2, max(nz, ny) - 1))] * 2,
-        *[pltpu.SemaphoreType.DMA((3, 2, 2, 4, PARTS))] * 2,
-        *ring,
-        *[pltpu.SemaphoreType.DMA((nx,))] * 2,
-        *[pltpu.SemaphoreType.DMA((nx - 1,))] * 2,
-        *[pltpu.SemaphoreType.DMA((max(ny - 1, 1),))] * 2,
+        *[pltpu.SemaphoreType.DMA((3,))] * 2,
+        pltpu.SemaphoreType.DMA((3,)),
+        pltpu.SemaphoreType.DMA((3, PARTS)),
+        pltpu.SemaphoreType.DMA((3, 2)),
+        pltpu.SemaphoreType.DMA,
+        pltpu.SemaphoreType.DMA((4,)),
+        *[pltpu.SemaphoreType.DMA] * 2,
+        *[pltpu.SemaphoreType.DMA] * 2,
+        *[pltpu.SemaphoreType.DMA] * 2,
         *[pltpu.SemaphoreType.DMA((max(nz - 1, 1),))] * 2,
-        *[pltpu.SemaphoreType.DMA((max(ny - 1, 1),))] * 2,
         *[pltpu.SemaphoreType.DMA] * 2,
-        *ring,
-        *ring,
-        *[pltpu.SemaphoreType.DMA((nx,))] * 2,
-        *[pltpu.SemaphoreType.DMA((nx - 1,))] * 2,
-        pltpu.SemaphoreType.DMA((17,)),
+        *[pltpu.SemaphoreType.DMA] * 2,
+        *[pltpu.SemaphoreType.DMA] * 2,
+        *[pltpu.SemaphoreType.DMA] * 2,
+        pltpu.SemaphoreType.DMA,
+        pltpu.SemaphoreType.DMA((nx,)),
+        *[pltpu.SemaphoreType.DMA] * 2,
+        pltpu.SemaphoreType.DMA((10,)),
     ]
     return pl.pallas_call(
         functools.partial(kernel, sizes),

time: 72.6 us -> 67.3 us (0.927)
  Pallas kernels: 70.8 us -> 65.4 us
    pallas_call x1, Pallas kernels: 70.8 us -> 65.4 us  [body(): pl.pallas_call(functools.partial(kernel, sizes), out_shape=jax.ShapeDtype...]
where the time goes in v3:
time: 67.3 us; the launch traced here: 67.1 us
  Pallas kernels  65.4 us (97%)
  local copies, waits for them, and re-layouts  1.67 us (2%)
    pallas_call x1, Pallas kernels, body(): pl.pallas_call(functools.partial(kernel, sizes), out_shape=jax.ShapeDtype...  65.4 us
    unnamed x1, local copies, waits for them, and re-layouts  1.67 us

profile of v3, /device:TPU:1, one launch (start us, length us, event | category | flops | bytes accessed | tf_op | source)
XLA Modules:
  0.0 67.1 jit_solution(3269788919464330408)
XLA Ops:
  0.0 65.4 %layer.1 = bf16[1,64,2048]{2,1,0:T(8,128)(2,1)} custom-call(bf16[1,64,2048]{2,1,0:T(8,128)(2,1)} %tok_hbm.1, f32[1,2048]{1,0:T(1,128)} %bitcast.9, bf16[32,512]{1,0:T(8,128)(2,1)} %wp_hbm.1, bf16[32,512]{1,0:T(8,128)(2,1)} %wq_hbm.1, bf16[32,512]{1,0:T(8,128)(2,1)} %wf_hbm.1, bf16[32,512]{1,0:T(8,128)(2,1)} %wv_hbm.1, bf16[2,256,256]{2,1,0:T(8,128)(2,1)} %maps_hbm.1, ...), custom_call_target="tpu_custom_call" | custom-call | tf_op jit(solution)/shard_map/layer/pallas_call | solution.py:744
  65.4 1.7 %copy.15 = bf16[1,64,2048]{2,1,0:T(8,128)(2,1)} copy(bf16[1,64,2048]{2,1,0:T(8,128)(2,1)} %layer.1) | data formatting | bytes 524288

commit v4 on v3

--- a/solution.py
+++ b/solution.py
@@ -496,6 +496,61 @@
     def _():
         halo[...] = jnp.zeros_like(halo)
 
+    def add_row(zz, carry):
+        if nz > 1:
+            rc(
+                c2_send, c2_recv.at[zz], c2_ss.at[z - zz - 1], c2_rs.at[z - zz - 1], z=zz
+            ).wait_recv()
+        block = c2_recv[zz].astype(F32)
+        out = []
+        for s in range(nx):
+            out.append(
+                read_decay(block, s) * carry[s] + block[s * piece : (s + 1) * piece, :]
+            )
+        return tuple(out)
+
+    earlier = tuple(jnp.zeros((piece, HEAD), F32) for _ in range(nx))
+    if nz > 1:
+        earlier = lax.fori_loop(0, z, add_row, earlier)
+    for j in range(ny):
+        for s in range(nx):
+            span = slice(s * piece, (s + 1) * piece)
+            c3_send[j, span, :] = (dex[j, s : s + 1, :] * earlier[s] + pex[j, span, :]).astype(BF16)
+    c3_recv[y] = c3_send[y]
+
+    def c3(k, slot):
+        to = at(y, k, ny)
+        return rc(c3_send.at[to], c3_recv.at[slot], c3_ss, c3_rs, y=to)
+
+    for k in far_first(ny):
+        c3(k, y).start()
+
+    if ny > 1:
+
+        @pl.when(y > 0)
+        def _():
+            halo_copy(y=y - 1).wait_recv()
+
+    if nz > 1:
+
+        @pl.when(jnp.logical_and(y == 0, z > 0))
+        def _():
+            halo_copy(z=z - 1, y=ny - 1).wait_recv()
+
+    group = (c * half_pool + x * HEAD) // WCOLS
+    window = jnp.where(group == 0, 2, jnp.where(group == 1, 4, jnp.where(group == 2, 8, 16)))
+    band = jnp.logical_and(ti >= si, ti - si < window).astype(BF16)
+    hi = lax.broadcasted_iota(jnp.int32, (TOK, HALO), 0)
+    hj = lax.broadcasted_iota(jnp.int32, (TOK, HALO), 1)
+    band_before = (hi + HALO - hj < window).astype(BF16)
+    place = sp * TOK + lax.broadcasted_iota(jnp.int32, (TOK, HEAD), 0) + 1
+    count = jnp.minimum(place, window).astype(F32)
+    for s in range(nx):
+        sums = nn(band, pbuf[s]) + nn(band_before, halo[s])
+        xpool[x, s * TOK : (s + 1) * TOK, :] = (sums / count - pbuf[s].astype(F32)).astype(BF16)
+
+    to_all_x(lambda owner: xpool.at[owner], xp_ss, xp_rs)
+
     p2_wait(1, (0,))
     qbuf[...] = project(wqp[0].reshape(width, HEAD))
 
@@ -516,61 +571,6 @@
         chosen = jnp.where(causal, scores[:, :TOK], jnp.where(before, cross, 0.0))
         within[span, :] = nn(chosen.astype(BF16), vbuf[span, :])
         cfull[span, :] = reader * jnp.exp(cfull[span, :])
-    if ny > 1:
-
-        @pl.when(y > 0)
-        def _():
-            halo_copy(y=y - 1).wait_recv()
-
-    if nz > 1:
-
-        @pl.when(jnp.logical_and(y == 0, z > 0))
-        def _():
-            halo_copy(z=z - 1, y=ny - 1).wait_recv()
-
-    group = (c * half_pool + x * HEAD) // WCOLS
-    window = jnp.where(group == 0, 2, jnp.where(group == 1, 4, jnp.where(group == 2, 8, 16)))
-    band = jnp.logical_and(ti >= si, ti - si < window).astype(BF16)
-    hi = lax.broadcasted_iota(jnp.int32, (TOK, HALO), 0)
-    hj = lax.broadcasted_iota(jnp.int32, (TOK, HALO), 1)
-    band_before = (hi + HALO - hj < window).astype(BF16)
-    place = sp * TOK + lax.broadcasted_iota(jnp.int32, (TOK, HEAD), 0) + 1
-    count = jnp.minimum(place, window).astype(F32)
-    for s in range(nx):
-        sums = nn(band, pbuf[s]) + nn(band_before, halo[s])
-        xpool[x, s * TOK : (s + 1) * TOK, :] = (sums / count - pbuf[s].astype(F32)).astype(BF16)
-
-    to_all_x(lambda owner: xpool.at[owner], xp_ss, xp_rs)
-
-    def add_row(zz, carry):
-        if nz > 1:
-            rc(
-                c2_send, c2_recv.at[zz], c2_ss.at[z - zz - 1], c2_rs.at[z - zz - 1], z=zz
-            ).wait_recv()
-        block = c2_recv[zz].astype(F32)
-        out = []
-        for s in range(nx):
-            out.append(
-                read_decay(block, s) * carry[s] + block[s * piece : (s + 1) * piece, :]
-            )
-        return tuple(out)
-
-    earlier = tuple(jnp.zeros((piece, HEAD), F32) for _ in range(nx))
-    if nz > 1:
-        earlier = lax.fori_loop(0, z, add_row, earlier)
-    for j in range(ny):
-        for s in range(nx):
-            span = slice(s * piece, (s + 1) * piece)
-            c3_send[j, span, :] = (dex[j, s : s + 1, :] * earlier[s] + pex[j, span, :]).astype(BF16)
-    c3_recv[y] = c3_send[y]
-
-    def c3(k, slot):
-        to = at(y, k, ny)
-        return rc(c3_send.at[to], c3_recv.at[slot], c3_ss, c3_rs, y=to)
-
-    for k in far_first(ny):
-        c3(k, y).start()
-
     p2_relay(2)
     taken(c3_rs, c3_send.at[0 : ny - 1])
     gain = hg_ref[pl.ds(x, 1), :]
@@ -748,10 +748,10 @@
         out_specs=pl.BlockSpec(memory_space=pltpu.VMEM),
         scratch_shapes=scratch,
         compiler_params=pltpu.CompilerParams(
-            collective_id=0, has_side_effects=True, vmem_limit_bytes=56 * 1024 * 1024
+            collective_id=0, has_side_effects=True, vmem_limit_bytes=40 * 1024 * 1024
         ),
         name="layer",
-    )(
+    )(*map(pinned, (
         tok,
         gin.reshape(1, width),
         wp,
@@ -765,7 +765,11 @@
         hg.reshape(nx, HEAD),
         wpo.T,
         wro.T,
-    )
+    )))
+
+
+def pinned(array):
+    return pltpu.with_memory_space_constraint(array, pltpu.HBM)
 
 
 def layout(devices, sizes):

time: 67.3 us -> 63.1 us (0.938); the launches traced: 67.1 us -> 62.1 us
  Pallas kernels: 65.4 us -> 61.4 us
  local copies, waits for them, and re-layouts: 1.67 us -> 0.71 us
    pallas_call x1, Pallas kernels: 65.4 us -> 61.4 us  [body(): pl.pallas_call(functools.partial(kernel, sizes), out_shape=jax.ShapeDtype...]
    unnamed x1, local copies, waits for them, and re-layouts: 1.67 us -> 0.71 us
where the time goes in v4:
time: 63.1 us; the launch traced here: 62.1 us
  Pallas kernels  61.4 us (97%)
  local copies, waits for them, and re-layouts  0.71 us (1%)
    pallas_call x1, Pallas kernels, body(): pl.pallas_call(functools.partial(kernel, sizes), out_shape=jax.ShapeDtype...  61.4 us

profile of v4, /device:TPU:1, one launch (start us, length us, event | category | flops | bytes accessed | tf_op | source)
XLA Modules:
  0.0 62.1 jit_solution(11655540954463207505)
XLA Ops:
  0.0 61.4 %layer.1 = bf16[1,64,2048]{2,1,0:T(8,128)(2,1)S(1)} custom-call(bf16[1,64,2048]{2,1,0:T(8,128)(2,1)} %tok_hbm.1, f32[1,2048]{1,0:T(1,128)} %bitcast.9, bf16[32,512]{1,0:T(8,128)(2,1)} %wp_hbm.1, bf16[32,512]{1,0:T(8,128)(2,1)} %wq_hbm.1, bf16[32,512]{1,0:T(8,128)(2,1)} %wf_hbm.1, bf16[32,512]{1,0:T(8,128)(2,1)} %wv_hbm.1, bf16[2,256,256]{2,1,0:T(8,128)(2,1)} %maps_hbm.1, ...), custom_call_target="tpu_custom_call" | custom-call | tf_op jit(solution)/shard_map/layer/pallas_call | solution.py:744
  61.4 0.7 %copy.15 = bf16[1,64,2048]{2,1,0:T(8,128)(2,1)} copy(bf16[1,64,2048]{2,1,0:T(8,128)(2,1)S(1)} %layer.1) | data formatting | bytes 524288

commit v5 on v4

--- a/solution.py
+++ b/solution.py
@@ -96,6 +96,7 @@
     part_in,
     mixed,
     obuf,
+    order,
     p1_ss,
     p1_rs,
     p2_ss,
@@ -275,8 +276,8 @@
         return [(path, way, part) for path in range(2) for way in range(2)]
 
     def p2_own(st):
-        for part in range(PARTS):
-            for distance in (2, 1):
+        for distance in (2, 1):
+            for part in range(PARTS):
                 for path, way, _ in each(part):
                     p2(st, path, way, 0, distance, part).start()
 
@@ -496,6 +497,23 @@
     def _():
         halo[...] = jnp.zeros_like(halo)
 
+    group = (c * half_pool + x * HEAD) // WCOLS
+    window = jnp.where(group == 0, 2, jnp.where(group == 1, 4, jnp.where(group == 2, 8, 16)))
+    band = jnp.logical_and(ti >= si, ti - si < window).astype(BF16)
+    hi = lax.broadcasted_iota(jnp.int32, (HALO, HALO), 0)
+    hj = lax.broadcasted_iota(jnp.int32, (HALO, HALO), 1)
+    band_before = (hi + HALO - hj < window).astype(BF16)
+    place = sp * TOK + lax.broadcasted_iota(jnp.int32, (TOK, HEAD), 0) + 1
+    count = jnp.minimum(place, window).astype(F32)
+
+    def pooled(sums, s, span):
+        return (sums / count[span] - pbuf[s, span, :].astype(F32)).astype(BF16)
+
+    for s in range(nx):
+        sums = nn(band, pbuf[s])
+        xpool[x, s, HALO:, :] = pooled(sums[HALO:], s, slice(HALO, TOK))
+    to_all_x(lambda owner: xpool.at[owner, :, HALO:TOK], xp_ss, xp_rs)
+
     def add_row(zz, carry):
         if nz > 1:
             rc(
@@ -537,19 +555,10 @@
         def _():
             halo_copy(z=z - 1, y=ny - 1).wait_recv()
 
-    group = (c * half_pool + x * HEAD) // WCOLS
-    window = jnp.where(group == 0, 2, jnp.where(group == 1, 4, jnp.where(group == 2, 8, 16)))
-    band = jnp.logical_and(ti >= si, ti - si < window).astype(BF16)
-    hi = lax.broadcasted_iota(jnp.int32, (TOK, HALO), 0)
-    hj = lax.broadcasted_iota(jnp.int32, (TOK, HALO), 1)
-    band_before = (hi + HALO - hj < window).astype(BF16)
-    place = sp * TOK + lax.broadcasted_iota(jnp.int32, (TOK, HEAD), 0) + 1
-    count = jnp.minimum(place, window).astype(F32)
     for s in range(nx):
-        sums = nn(band, pbuf[s]) + nn(band_before, halo[s])
-        xpool[x, s * TOK : (s + 1) * TOK, :] = (sums / count - pbuf[s].astype(F32)).astype(BF16)
-
-    to_all_x(lambda owner: xpool.at[owner], xp_ss, xp_rs)
+        sums = nn(band[:HALO], pbuf[s]) + nn(band_before, halo[s])
+        xpool[x, s, :HALO, :] = pooled(sums, s, slice(0, HALO))
+    to_all_x(lambda owner: xpool.at[owner, :, 0:HALO], xp_ss, xp_rs)
 
     p2_wait(1, (0,))
     qbuf[...] = project(wqp[0].reshape(width, HEAD))
@@ -572,6 +581,16 @@
         within[span, :] = nn(chosen.astype(BF16), vbuf[span, :])
         cfull[span, :] = reader * jnp.exp(cfull[span, :])
     p2_relay(2)
+    chunk = min(HEAD, (nz * ny * wo_cols))
+    total_cols = chunk * nx
+    src = lax.broadcasted_iota(jnp.int32, (total_cols, total_cols), 0)
+    dst = lax.broadcasted_iota(jnp.int32, (total_cols, total_cols), 1)
+    wanted = (
+        lax.div(lax.rem(dst, 32), wo_cols) * chunk
+        + lax.div(dst, 32) * wo_cols
+        + lax.rem(dst, wo_cols)
+    )
+    order[...] = (src == wanted).astype(BF16)
     taken(c3_rs, c3_send.at[0 : ny - 1])
     gain = hg_ref[pl.ds(x, 1), :]
 
@@ -590,7 +609,9 @@
     pieces = []
     for g in range(half_pool // WCOLS):
         cols = slice(g * WCOLS, (g + 1) * WCOLS)
-        diff = jnp.concatenate([xpool[2 * g], xpool[2 * g + 1]], axis=1)
+        diff = jnp.concatenate(
+            [xpool[2 * g + n].reshape(rows, HEAD) for n in range(2)], axis=1
+        )
         pieces.append((nn(diff, maps_ref[g]) * scale_ref[:, cols]).astype(BF16))
     p2_wait(2)
     for p in range(2):
@@ -631,20 +652,13 @@
             obuf[x] = joint
     taken(o_rs, mixed.at[0 : nx - 1])
 
-    chunk = min(HEAD, cols_out)
-    total_cols = chunk * nx
-    src = lax.broadcasted_iota(jnp.int32, (total_cols, total_cols), 0)
-    dst = lax.broadcasted_iota(jnp.int32, (total_cols, total_cols), 1)
-    wanted = (
-        lax.div(lax.rem(dst, 32), wo_cols) * chunk
-        + lax.div(dst, 32) * wo_cols
-        + lax.rem(dst, wo_cols)
-    )
-    order = (src == wanted).astype(BF16)
+    joined = [
+        jnp.concatenate([obuf[i, :, q * chunk : (q + 1) * chunk] for i in range(nx)], axis=1)
+        for q in range(cols_out // chunk)
+    ]
+    ordered = nn(jnp.concatenate(joined, axis=0), order[...]).astype(BF16)
     for q in range(cols_out // chunk):
-        cols = slice(q * chunk, (q + 1) * chunk)
-        joined = jnp.concatenate([obuf[i, :, cols] for i in range(nx)], axis=1)
-        out_ref[0, :, q * total_cols : (q + 1) * total_cols] = nn(joined, order).astype(BF16)
+        out_ref[0, :, q * total_cols : (q + 1) * total_cols] = ordered[q * HALF : (q + 1) * HALF]
 
     for st in range(3):
         p1_done(st)
@@ -715,13 +729,14 @@
         pltpu.VMEM((ny, packed, HEAD), BF16),
         pltpu.VMEM((nx, HALO, HEAD), BF16),
         pltpu.VMEM((rows, HEAD), F32),
-        pltpu.VMEM((nx, rows, HEAD), BF16),
+        pltpu.VMEM((nx, nx, TOK, HEAD), BF16),
         pltpu.VMEM((nx, nx, 2, HALF, HEAD), BF16),
         pltpu.VMEM((nx, 2, HALF, cols_out), F32),
         pltpu.VMEM((nx, 2, HALF, cols_out), BF16),
         pltpu.VMEM((nx, HALF, cols_out), BF16),
         pltpu.VMEM((nx, HALF, cols_out), BF16),
         pltpu.VMEM((nx, HALF, cols_out), BF16),
+        pltpu.VMEM((nx * min(HEAD, cols_out), nx * min(HEAD, cols_out)), BF16),
         *[pltpu.SemaphoreType.DMA((3,))] * 2,
         pltpu.SemaphoreType.DMA((3,)),
         pltpu.SemaphoreType.DMA((3, PARTS)),

time: 63.1 us -> 62.1 us (0.984); the launches traced: 62.1 us -> 62 us
  no operation moved by 1% of the time
where the time goes in v5:
time: 62.1 us; the launch traced here: 62 us
  Pallas kernels  61.3 us (99%)
  local copies, waits for them, and re-layouts  0.71 us (1%)
    pallas_call x1, Pallas kernels, body(): pl.pallas_call(functools.partial(kernel, sizes), out_shape=jax.ShapeDtype...  61.3 us

profile of v5, /device:TPU:1, one launch (start us, length us, event | category | flops | bytes accessed | tf_op | source)
XLA Modules:
  0.0 62.0 jit_solution(2918168078844793153)
XLA Ops:
  0.0 61.3 %layer.1 = bf16[1,64,2048]{2,1,0:T(8,128)(2,1)S(1)} custom-call(bf16[1,64,2048]{2,1,0:T(8,128)(2,1)} %tok_hbm.1, f32[1,2048]{1,0:T(1,128)} %bitcast.9, bf16[32,512]{1,0:T(8,128)(2,1)} %wp_hbm.1, bf16[32,512]{1,0:T(8,128)(2,1)} %wq_hbm.1, bf16[32,512]{1,0:T(8,128)(2,1)} %wf_hbm.1, bf16[32,512]{1,0:T(8,128)(2,1)} %wv_hbm.1, bf16[2,256,256]{2,1,0:T(8,128)(2,1)} %maps_hbm.1, ...), custom_call_target="tpu_custom_call" | custom-call | tf_op jit(solution)/shard_map/layer/pallas_call | solution.py:759
  61.3 0.7 %copy.15 = bf16[1,64,2048]{2,1,0:T(8,128)(2,1)} copy(bf16[1,64,2048]{2,1,0:T(8,128)(2,1)S(1)} %layer.1) | data formatting | bytes 524288

commit v6 on v5

--- a/solution.py
+++ b/solution.py
@@ -629,7 +629,7 @@
 
     def deliver(k, owner):
         to = at(x, k, nx)
-        return rc(mixed.at[to], obuf.at[owner], o_ss, o_rs, x=to)
+        return rc(mixed.at[to], obuf.at[owner], o_ss, o_rs.at[k - 1], x=to)
 
     order_x = (*far_first(nx), 0)
     def half_of(core):
@@ -650,13 +650,17 @@
             deliver(k, x).start()
         else:
             obuf[x] = joint
-    taken(o_rs, mixed.at[0 : nx - 1])
-
-    joined = [
-        jnp.concatenate([obuf[i, :, q * chunk : (q + 1) * chunk] for i in range(nx)], axis=1)
-        for q in range(cols_out // chunk)
-    ]
-    ordered = nn(jnp.concatenate(joined, axis=0), order[...]).astype(BF16)
+    def reordered(owner):
+        stacked = jnp.concatenate(
+            [obuf[owner, :, q * chunk : (q + 1) * chunk] for q in range(cols_out // chunk)], axis=0
+        )
+        return nn(stacked, order[pl.ds(pl.multiple_of(owner * chunk, chunk), chunk), :])
+
+    ordered = reordered(x)
+    for k in (1, 3, 2):
+        deliver(k, at(x, -k, nx)).wait_recv()
+        ordered = ordered + reordered(at(x, -k, nx))
+    ordered = ordered.astype(BF16)
     for q in range(cols_out // chunk):
         out_ref[0, :, q * total_cols : (q + 1) * total_cols] = ordered[q * HALF : (q + 1) * HALF]
 
@@ -753,7 +757,8 @@
         *[pltpu.SemaphoreType.DMA] * 2,
         pltpu.SemaphoreType.DMA,
         pltpu.SemaphoreType.DMA((nx,)),
-        *[pltpu.SemaphoreType.DMA] * 2,
+        pltpu.SemaphoreType.DMA,
+        pltpu.SemaphoreType.DMA((nx - 1,)),
         pltpu.SemaphoreType.DMA((10,)),
     ]
     return pl.pallas_call(

time: 62.1 us -> 62.3 us (level)
  no operation moved by 1% of the time
where the time goes in v6:
time: 62.3 us; the launch traced here: 62.2 us
  Pallas kernels  61.5 us (99%)
  local copies, waits for them, and re-layouts  0.71 us (1%)
    pallas_call x1, Pallas kernels, body(): pl.pallas_call(functools.partial(kernel, sizes), out_shape=jax.ShapeDtype...  61.5 us

profile of v6, /device:TPU:1, one launch (start us, length us, event | category | flops | bytes accessed | tf_op | source)
XLA Modules:
  0.0 62.2 jit_solution(10267311237863409442)
XLA Ops:
  0.0 61.5 %layer.1 = bf16[1,64,2048]{2,1,0:T(8,128)(2,1)S(1)} custom-call(bf16[1,64,2048]{2,1,0:T(8,128)(2,1)} %tok_hbm.1, f32[1,2048]{1,0:T(1,128)} %bitcast.9, bf16[32,512]{1,0:T(8,128)(2,1)} %wp_hbm.1, bf16[32,512]{1,0:T(8,128)(2,1)} %wq_hbm.1, bf16[32,512]{1,0:T(8,128)(2,1)} %wf_hbm.1, bf16[32,512]{1,0:T(8,128)(2,1)} %wv_hbm.1, bf16[2,256,256]{2,1,0:T(8,128)(2,1)} %maps_hbm.1, ...), custom_call_target="tpu_custom_call" | custom-call | tf_op jit(solution)/shard_map/layer/pallas_call | solution.py:764
  61.5 0.7 %copy.15 = bf16[1,64,2048]{2,1,0:T(8,128)(2,1)} copy(bf16[1,64,2048]{2,1,0:T(8,128)(2,1)S(1)} %layer.1) | data formatting | bytes 524288
